TPU v7x, 32 devices: a whole 2x2x4 slice. The times are simulated.
32 devices in a mesh: sp: 16 (over z, y, x), tp: 2 (over core).
Axes of the slice: x: 2, y: 2, z: 4, core: 2. Of those that a mesh axis runs over, the one named last changes fastest.
Arguments:
- stream: bfloat16 [4096, 2048], P(('sp', 'tp')), may hold values from -6 to 6
- head_input_signal: bfloat16 [4096, 2048], P('sp', 'tp'), may hold values from -6 to 6
- write_input_vectors: bfloat16 [4096, 512], P('sp', 'tp'), may hold values from -6 to 6
- read_input_vectors: bfloat16 [4096, 512], P('sp', 'tp'), may hold values from -6 to 6
- output_gate_input: bfloat16 [4096, 2048], P('sp', 'tp'), may hold values from -6 to 6
- step_size_input: bfloat16 [4096, 32], P('sp', 'tp'), may hold values from -5 to 5.5
- position_log_decay: float32 [4096, 32], P('sp', 'tp'), may hold values from -0.7 to 0
- signal_filter_taps: bfloat16 [4, 2048], P(None, 'tp'), may hold values from -3 to 3
- write_filter_taps: bfloat16 [4, 512], P(None, 'tp'), may hold values from -3 to 3
- read_filter_taps: bfloat16 [4, 512], P(None, 'tp'), may hold values from -3 to 3
- step_size_bias: float32 [32], P('tp'), may hold values from -1 to 1
- head_decay_rate: float32 [32], P('tp'), may hold values from 2.4414063e-06 to 0.03
- head_direct_term: float32 [32], P('tp'), may hold values from 0.5 to 2
- grouped_norm_gain: float32 [2048], P('tp'), may hold values from 0.1 to 1.9
- mixer_output_weight: bfloat16 [2048, 2048], P('tp'), may hold values from -0.125 to 0.125
- expert_norm_gain: float32 [2048], replicated, may hold values from 0.1 to 1.9
- chosen_expert_index: int32 [4096, 4], P(('sp', 'tp')), may hold values from 0 to 31, all different within a row; in each aligned block of 128 rows (0 to 127, 128 to 255, ...) at most 24 rows name the same one
- chosen_expert_weight: float32 [4096, 4], P(('sp', 'tp')), may hold values from 0.1 to 1
- routed_gate_weight: bfloat16 [32, 2048, 512], P(('sp', 'tp')), may hold values from -0.125 to 0.125
- routed_up_weight: bfloat16 [32, 2048, 512], P(('sp', 'tp')), may hold values from -0.125 to 0.125
- routed_down_weight: bfloat16 [32, 512, 2048], P(('sp', 'tp')), may hold values from -0.25 to 0.25
- common_gate_weight: bfloat16 [2048, 512], replicated, may hold values from -0.125 to 0.125
- common_up_weight: bfloat16 [2048, 512], replicated, may hold values from -0.125 to 0.125
- common_down_weight: bfloat16 [512, 2048], replicated, may hold values from -0.25 to 0.25
Outputs:
- layer_out: bfloat16 [4096, 2048], P(('sp', 'tp'))
Inputs may be any that keep to these rules, and one draw needn't show every extreme that they name: `chosen_expert_index`: each row names 4 different experts. Among the 128 rows of one device (aligned blocks of 128 rows) no expert is named more than 24 times; in some block one expert is named exactly 24 times.
All inputs are finite; a program needn't handle non-finite values.
Results may differ from a plain program's by a relative error of at most 0.015.
Values may be sent and summed in bfloat16 or wider, within the bound.
A program may use at most 128 MiB of HBM per device.

v0:
```python
import jax
import jax.numpy as jnp
from jax import lax
from jax.sharding import PartitionSpec as P

HEAD_DIM = 64
STATE = 128
BLK = 128


def from_behind(block, axis, distance):
    devices = range(lax.axis_size(axis))
    route = [(i - distance, i) for i in devices if i - distance in devices]
    return lax.ppermute(block, axis, route)


def swap(block, axis, step, upward_only):
    devices = range(lax.axis_size(axis))
    route = [(i, i ^ step) for i in devices if not (upward_only and i & step)]
    return lax.ppermute(block, axis, route)


def carried_in(log_total, state, axis):
    count, mine = lax.axis_size(axis), lax.axis_index(axis)
    heads, width = log_total.size, state.shape[-1]
    flat = state.reshape(heads, -1, width)
    decay = jnp.exp(log_total).reshape(heads)
    total, before, before_decay = flat, jnp.zeros_like(flat), jnp.ones_like(decay)
    step = 1
    while step < count:
        coarse = lax.reduce_precision(decay, 8, 7)
        lane = jnp.arange(width)[None, :]
        tail = jnp.where(lane == 0, coarse[:, None], jnp.where(lane == 1, (decay - coarse)[:, None], 0.0))
        sent = jnp.concatenate([total.reshape(-1, width), tail], axis=0).astype(jnp.bfloat16)
        got = swap(sent, axis, step, 2 * step >= count).astype(jnp.float32)
        other = got[: got.shape[0] - heads].reshape(flat.shape)
        other_decay = got[got.shape[0] - heads :, 0] + got[got.shape[0] - heads :, 1]
        upper = (mine & step) != 0
        before = before + jnp.where(upper, before_decay, 0.0)[:, None, None] * other
        if 2 * step < count:
            before_decay = before_decay * jnp.where(upper, other_decay, 1.0)
            total = jnp.where(
                upper, other * decay[:, None, None] + total, total * other_decay[:, None, None] + other
            )
            decay = decay * other_decay
        step *= 2
    return before.reshape(state.shape)


def causal_conv(previous, current, weight):
    stacked = jnp.concatenate([previous, current], axis=0).astype(jnp.float32)
    weight = weight.astype(jnp.float32)
    kernel_len = weight.shape[0]
    length = current.shape[0]
    summed_taps = weight[0] * stacked[0:length]
    for offset in range(1, kernel_len):
        summed_taps = summed_taps + weight[offset] * stacked[offset : offset + length]
    return jax.nn.silu(summed_taps)


def product(spec, *operands):
    return jnp.einsum(
        spec, *[part.astype(jnp.bfloat16) for part in operands], preferred_element_type=jnp.float32
    )


def on_device(
    stream,
    head_input_signal,
    write_input_vectors,
    read_input_vectors,
    output_gate_input,
    step_size_input,
    position_log_decay,
    signal_filter_taps,
    write_filter_taps,
    read_filter_taps,
    step_size_bias,
    head_decay_rate,
    head_direct_term,
    grouped_norm_gain,
    mixer_output_weight,
    expert_norm_gain,
    chosen_expert_index,
    chosen_expert_weight,
    routed_gate_weight,
    routed_up_weight,
    routed_down_weight,
    common_gate_weight,
    common_up_weight,
    common_down_weight,
):
    length = head_input_signal.shape[0]
    margin = signal_filter_taps.shape[0] - 1
    head_count = step_size_input.shape[1]
    groups = write_input_vectors.shape[1] // STATE
    per_group = head_count // groups
    blocks = length // BLK
    wide, narrow = head_input_signal.shape[1], write_input_vectors.shape[1]
    rim = jnp.concatenate(
        [part[length - margin :] for part in (head_input_signal, write_input_vectors, read_input_vectors)],
        axis=1,
    )
    rim = from_behind(rim, "sp", 1)
    before = (rim[:, :wide], rim[:, wide : wide + narrow], rim[:, wide + narrow :])
    signal = causal_conv(before[0], head_input_signal, signal_filter_taps)
    write_vec = causal_conv(before[1], write_input_vectors, write_filter_taps)
    read_vec = causal_conv(before[2], read_input_vectors, read_filter_taps)
    time_position = jax.nn.softplus(step_size_input.astype(jnp.float32) + step_size_bias)
    decay_logarithm = position_log_decay - head_decay_rate * time_position
    signal_heads = signal.reshape(blocks, BLK, groups, per_group, HEAD_DIM)
    scaled_blocks = signal_heads * time_position.reshape(blocks, BLK, groups, per_group)[..., None]
    write_blocks = write_vec.reshape(blocks, BLK, groups, STATE)
    read_blocks = read_vec.reshape(blocks, BLK, groups, STATE)
    within_cum = jnp.cumsum(decay_logarithm.reshape(blocks, BLK, groups, per_group), axis=1)
    block_total = within_cum[:, -1]
    running = jnp.cumsum(block_total, axis=0)
    device_total = running[-1]
    causal = jnp.arange(BLK)[:, None] >= jnp.arange(BLK)[None, :]
    cum_heads = jnp.transpose(within_cum, (0, 2, 3, 1))
    differences = cum_heads[..., :, None] - cum_heads[..., None, :]
    decay_matrix = jnp.exp(jnp.where(causal, differences, -jnp.inf))
    tail_decay = jnp.exp(block_total[:, None] - within_cum)
    block_states = product(
        "bsgn,bsgep->bgepn", write_blocks, scaled_blocks * tail_decay[..., None]
    )
    device_state = jnp.sum(
        block_states * jnp.exp(device_total[None] - running)[..., None, None], axis=0
    )
    incoming = carried_in(device_total, device_state, "sp")
    intersection = product("btgn,bsgn->bgts", read_blocks, write_blocks)
    intra_out = product(
        "bgets,bsgep->btgep", intersection[:, :, None] * decay_matrix, scaled_blocks
    )
    readout_scale = jnp.exp(within_cum)
    starts = [incoming]
    for block in range(blocks - 1):
        starts.append(
            starts[-1] * jnp.exp(block_total[block])[..., None, None] + block_states[block]
        )
    near_out = (
        product("btgn,bgepn->btgep", read_blocks, jnp.stack(starts)) * readout_scale[..., None]
    )
    ssd_out = intra_out + near_out
    ssd_out = ssd_out + head_direct_term.reshape(groups, per_group)[:, :, None] * signal_heads
    gated = ssd_out.reshape(length, groups, per_group * HEAD_DIM) * jax.nn.silu(
        output_gate_input.astype(jnp.float32)
    ).reshape(length, groups, per_group * HEAD_DIM)
    norm_scale = lax.rsqrt(jnp.mean(gated * gated, axis=-1, keepdims=True) + 1e-06)
    mixer_out = ((gated * norm_scale).reshape(length, -1) * grouped_norm_gain).astype(jnp.bfloat16)
    row_count = stream.shape[0]
    tp_count = lax.axis_size("tp")
    core = lax.axis_index("tp")

    def share_of(owner):
        rows = lax.dynamic_slice_in_dim(mixer_out, owner * row_count, row_count, 0)
        return jnp.dot(rows, mixer_output_weight, preferred_element_type=jnp.float32)

    shares = []
    for ahead in range(1, tp_count):
        route = [(i, (i + ahead) % tp_count) for i in range(tp_count)]
        part = share_of((core + ahead) % tp_count).astype(jnp.bfloat16)
        shares.append(lax.ppermute(part, "tp", route))
    summed = share_of(core)
    for part in shares:
        summed = summed + part.astype(jnp.float32)
    residual = (stream.astype(jnp.float32) + summed).astype(jnp.bfloat16)
    widened = residual.astype(jnp.float32)
    normed = (
        widened
        * lax.rsqrt(jnp.mean(widened * widened, axis=-1, keepdims=True) + 1e-06)
        * expert_norm_gain
    ).astype(jnp.bfloat16)
    shared_hidden = (
        jax.nn.silu(jnp.dot(normed, common_gate_weight, preferred_element_type=jnp.float32))
        * jnp.dot(normed, common_up_weight, preferred_element_type=jnp.float32)
    ).astype(jnp.bfloat16)
    shared = jnp.dot(shared_hidden, common_down_weight, preferred_element_type=jnp.float32)
    sp_count = lax.axis_size("sp")
    experts = sp_count * tp_count
    fanout = chosen_expert_index.shape[1]
    capacity = max(2, (3 * row_count * fanout + 2 * experts - 1) // (2 * experts))
    named = chosen_expert_index[:, :, None] == jnp.arange(experts, dtype=jnp.int32)
    hits = jnp.any(named, axis=1)
    share = jnp.sum(jnp.where(named, chosen_expert_weight[:, :, None], 0.0), axis=1)
    ahead = (jnp.arange(row_count)[:, None] > jnp.arange(row_count)[None, :]).astype(jnp.bfloat16)
    slot = jnp.dot(ahead, hits.astype(jnp.bfloat16), preferred_element_type=jnp.float32)
    slot = jnp.where(hits, slot.astype(jnp.int32), -1)
    places = jnp.arange(capacity, dtype=jnp.int32)
    half = experts // 2
    side = lax.axis_index("sp") // (sp_count // 2)
    sides = [list(range(half)), list(range(half, experts))]
    across = sp_count // 2
    tables = jnp.stack([slot.astype(jnp.float32), share])
    near_table = lax.dynamic_slice_in_dim(tables, side * half, half, 2)
    far_table = swap(
        lax.dynamic_slice_in_dim(tables, (1 - side) * half, half, 2), "sp", across, False
    )

    def exchange(block):
        return lax.all_to_all(
            block,
            ("sp", "tp"),
            split_axis=0,
            concat_axis=0,
            axis_index_groups=sides,
            tiled=True,
        )

    def dispatch(table, rows):
        slots = table[0].astype(jnp.int32)
        pick = slots.T[:, None, :] == places[None, :, None]
        pick = pick.reshape(half * capacity, row_count).astype(jnp.bfloat16)
        picked = jnp.dot(pick, rows, preferred_element_type=jnp.float32)
        return exchange(picked.astype(jnp.bfloat16).reshape(half, capacity, -1))

    def expert(arrived):
        flat_rows = arrived.reshape(half * capacity, -1)
        hidden = (
            jax.nn.silu(
                jnp.dot(flat_rows, routed_gate_weight[0], preferred_element_type=jnp.float32)
            )
            * jnp.dot(flat_rows, routed_up_weight[0], preferred_element_type=jnp.float32)
        ).astype(jnp.bfloat16)
        result = jnp.dot(hidden, routed_down_weight[0], preferred_element_type=jnp.float32)
        return result.astype(jnp.bfloat16).reshape(arrived.shape)

    def collect(table, returned):
        slots = table[0].astype(jnp.int32)
        spread = jnp.where(slots[:, :, None] == places, table[1][:, :, None], 0.0)
        spread = spread.reshape(row_count, half * capacity)
        coarse = lax.reduce_precision(spread, 8, 7)
        fine = (spread - coarse).astype(jnp.bfloat16)
        back = returned.reshape(half * capacity, -1)
        return jnp.dot(
            coarse.astype(jnp.bfloat16), back, preferred_element_type=jnp.float32
        ) + jnp.dot(fine, back, preferred_element_type=jnp.float32)

    far_rows = swap(normed, "sp", across, False)
    near_rows = dispatch(near_table, normed)
    near_rows, far_rows = lax.optimization_barrier((near_rows, far_rows))
    far_arrived = dispatch(far_table, far_rows)
    near_out = expert(near_rows)
    far_out = expert(far_arrived)
    far_sum = collect(far_table, exchange(far_out)).astype(jnp.bfloat16)
    near_out, far_sum = lax.optimization_barrier((near_out, far_sum))
    from_far = swap(far_sum, "sp", across, False)
    near_sum = collect(near_table, exchange(near_out))
    return (widened + shared + near_sum + from_far.astype(jnp.float32)).astype(jnp.bfloat16)


def solution(mesh):
    in_specs = (
        P(("sp", "tp"), None),
        P("sp", "tp"),
        P("sp", "tp"),
        P("sp", "tp"),
        P("sp", "tp"),
        P("sp", "tp"),
        P("sp", "tp"),
        P(None, "tp"),
        P(None, "tp"),
        P(None, "tp"),
        P("tp"),
        P("tp"),
        P("tp"),
        P("tp"),
        P("tp", None),
        P(),
        P(("sp", "tp"), None),
        P(("sp", "tp"), None),
        P(("sp", "tp"), None, None),
        P(("sp", "tp"), None, None),
        P(("sp", "tp"), None, None),
        P(),
        P(),
        P(),
    )
    out_specs = P(("sp", "tp"), None)
    return jax.shard_map(
        on_device, mesh=mesh, in_specs=in_specs, out_specs=out_specs, check_vma=False
    )
```

profile of v0, /device:TPU:0, one launch (start us, length us, event | category | flops | bytes accessed | tf_op | source)
XLA Modules:
  0.0 270.2 jit_solution(17647930401037355570)
XLA Ops:
  3.2 5.6 %collective-permute-start = (bf16[3,1536]{0,1:T(8,128)(2,1)}, bf16[3,1536]{0,1:T(8,128)(2,1)}, u32[]{:S(2)}, u32[]{:S(2)}) collective-permute-start(bf16[3,1536]{0,1:T(8,128)(2,1)} %copy.131), channel_id=1, source_target_pairs={{0,2},{2,4},{4,6},{6,8},{8,10},{10,12},{12,14},{14,16},{16,18},{18... | collective-permute-start | bytes 27656 | tf_op jit(solution)/shard_map/ppermute | solution.py:14
  18.6 2.4 divide_multiply_fusion
  27.1 2.1 multiply_reduce_fusion
  30.7 2.0 collective-permute-start.1
  35.6 2.0 copy.149
  37.6 2.3 convert_multiply_fusion.2
  45.9 2.5 fusion.155
  53.6 2.7 %reshape.439 = f32[2,128,2,8,64]{1,0,4,3,2:T(2,128)} reshape(f32[256,1024]{0,1:T(8,128)} %convert_multiply_fusion.2) | data formatting | bytes 2097152 | tf_op jit(solution)/shard_map/reshape | solution.py:148
  84.6 2.3 select_convert_fusion
  87.0 5.2 %collective-permute-start.4 = (bf16[1040,128]{1,0:T(8,128)(2,1)S(1)}, bf16[1040,128]{1,0:T(8,128)(2,1)}, u32[]{:S(2)}, u32[]{:S(2)}) collective-permute-start(bf16[1040,128]{1,0:T(8,128)(2,1)S(1)} %pad_maximum_fusion.3), channel_id=1, source_target_pairs={{0,16},{2,18},{4,20},{6,22},{8,24},{10,26},{12,28},{14,30},{1,17},... | collective-permute-start | bytes 798728 | tf_op jit(solution)/shard_map/ppermute | solution.py:20
  92.2 2.7 convolution_bitcast_fusion.5
  105.7 4.2 %collective-permute-done.7 = f32[2,128,16]{1,2,0:T(8,128)S(1)} collective-permute-done((f32[2,128,16]{1,2,0:T(8,128)S(1)}, f32[2,128,16]{1,2,0:T(8,128)S(1)}, u32[]{:S(2)}, u32[]{:S(2)}) %collective-permute-start.7) | collective-permute-done | bytes 16416 | tf_op jit(solution)/shard_map/ppermute | solution.py:20
  110.0 3.3 %fusion.38 = (f32[128]{0:T(128)S(1)}, bf16[128,2048]{1,0:T(8,128)(2,1)S(1)}) fusion(bf16[128,2048]{1,0:T(8,128)(2,1)} %collective-permute-done.5, bf16[1024,2048]{1,0:T(8,128)(2,1)} %param.38, bf16[256,1024]{0,1:T(8,128)(2,1)} %copy-done.9, s32[]{:T(128)S(6)} %select_n.214, bf16[128,2048]{1,0:T(8,128)(2,1)S(1)} %copy-done.12), kind=kOutput, calls=%fused_computation.49 | convolution fusion | flops 538967936 | bytes 6029828 | tf_op jit(solution)/shard_map/dot_general | solution.py:157
  115.1 7.1 %all-to-all-start = ((bf16[16,24,2048]{2,1,0:T(8,128)(2,1)}), bf16[16,24,2048]{2,1,0:T(8,128)(2,1)}, u32[]{:S(2)}, u32[]{:S(2)}) async-start(bf16[16,24,2048]{2,1,0:T(8,128)(2,1)} %bitcast.158), calls=%async_computation | async-start | bytes 3145728 | tf_op jit(solution)/shard_map/all_to_all | solution.py:201
  122.4 3.0 %collective-permute-start.6 = (bf16[128,2048]{1,0:T(8,128)(2,1)S(1)}, bf16[128,2048]{1,0:T(8,128)(2,1)}, u32[]{:S(2)}, u32[]{:S(2)}) collective-permute-start(bf16[128,2048]{1,0:T(8,128)(2,1)S(1)} %fusion.40), channel_id=1, source_target_pairs={{0,16},{2,18},{4,20},{6,22},{8,24},{10,26},{12,28},{14,30},{16,0},... | collective-permute-start | bytes 1572872 | tf_op jit(solution)/shard_map/ppermute | solution.py:20
  125.4 26.6 %collective-permute-done.6 = bf16[128,2048]{1,0:T(8,128)(2,1)} collective-permute-done((bf16[128,2048]{1,0:T(8,128)(2,1)S(1)}, bf16[128,2048]{1,0:T(8,128)(2,1)}, u32[]{:S(2)}, u32[]{:S(2)}) %collective-permute-start.6) | collective-permute-done | bytes 524320 | tf_op jit(solution)/shard_map/ppermute | solution.py:20
  152.0 3.6 %all-to-all-done = bf16[16,24,2048]{2,1,0:T(8,128)(2,1)} async-done(((bf16[16,24,2048]{2,1,0:T(8,128)(2,1)}), bf16[16,24,2048]{2,1,0:T(8,128)(2,1)}, u32[]{:S(2)}, u32[]{:S(2)}) %all-to-all-start) | async-done | bytes 1572896 | tf_op jit(solution)/shard_map/all_to_all | solution.py:201
  157.2 26.4 %all_to_all.20 = bf16[16,24,2048]{2,1,0:T(8,128)(2,1)S(1)} all-to-all(bf16[16,24,2048]{2,1,0:T(8,128)(2,1)S(1)} %bitcast.159), channel_id=1, replica_groups={{0,1,2,3,4,5,6,7,8,9,10,11,12,13,14,15},{16,17,18,19,20,21,22,23,24,25,..., dimensions={0} | all-to-all | bytes 3145728 | tf_op jit(solution)/shard_map/all_to_all | solution.py:201
  184.8 1.9 fusion.10
  186.7 5.3 %convolution_convert_fusion = bf16[384,2048]{1,0:T(8,128)(2,1)} fusion(bf16[1,512,2048]{2,1,0:T(8,128)(2,1)S(1)} %copy-done, bf16[384,2048]{1,0:T(8,128)(2,1)} %bitcast.168, bf16[1,2048,512]{2,1,0:T(8,128)(2,1)} %param.43, f32[384,512]{1,0:T(8,128)} %fusion.10), kind=kOutput, calls=%fused_computation | convolution fusion | flops 1612578816 | bytes 8126464 | tf_op jit(solution)/shard_map/dot_general | solution.py:225
  191.9 4.4 %all-to-all-start.2 = ((bf16[16,24,2048]{2,1,0:T(8,128)(2,1)}), bf16[16,24,2048]{2,1,0:T(8,128)(2,1)}, u32[]{:S(2)}, u32[]{:S(2)}) async-start(bf16[16,24,2048]{2,1,0:T(8,128)(2,1)} %bitcast.166), calls=%async_computation.2 | async-start | bytes 3145728 | tf_op jit(solution)/shard_map/all_to_all | solution.py:201
  196.3 4.0 %fusion.12 = f32[384,512]{1,0:T(8,128)} fusion(bf16[384,2048]{1,0:T(8,128)(2,1)} %bitcast.36, bf16[1,2048,512]{2,1,0:T(8,128)(2,1)} %param.42), kind=kOutput, calls=%fused_computation.22 | convolution fusion | flops 805306368 | bytes 4456448 | tf_op jit(solution)/shard_map/dot_general | solution.py:221
  200.3 5.3 %convolution_convert_fusion.2 = bf16[384,2048]{1,0:T(8,128)(2,1)} fusion(bf16[1,512,2048]{2,1,0:T(8,128)(2,1)S(1)} %copy-done, bf16[384,2048]{1,0:T(8,128)(2,1)} %bitcast.36, bf16[1,2048,512]{2,1,0:T(8,128)(2,1)} %param.43, f32[384,512]{1,0:T(8,128)} %fusion.12), kind=kOutput, calls=%fused_computation.2 | convolution fusion | flops 1612578816 | bytes 8126464 | tf_op jit(solution)/shard_map/dot_general | solution.py:225
  205.6 13.2 %all-to-all-done.2 = bf16[16,24,2048]{2,1,0:T(8,128)(2,1)} async-done(((bf16[16,24,2048]{2,1,0:T(8,128)(2,1)}), bf16[16,24,2048]{2,1,0:T(8,128)(2,1)}, u32[]{:S(2)}, u32[]{:S(2)}) %all-to-all-start.2) | async-done | bytes 1572896 | tf_op jit(solution)/shard_map/all_to_all | solution.py:201
  218.9 1.9 convolution_bitcast_fusion.2
  220.8 2.7 fusion.3
  223.4 4.4 %all-to-all-start.3 = ((bf16[16,24,2048]{2,1,0:T(8,128)(2,1)}), bf16[16,24,2048]{2,1,0:T(8,128)(2,1)}, u32[]{:S(2)}, u32[]{:S(2)}) async-start(bf16[16,24,2048]{2,1,0:T(8,128)(2,1)} %bitcast.165), calls=%async_computation.3 | async-start | bytes 3145728 | tf_op jit(solution)/shard_map/all_to_all | solution.py:201
  229.2 2.1 fusion.149
  231.2 29.7 %all-to-all-done.3 = bf16[16,24,2048]{2,1,0:T(8,128)(2,1)} async-done(((bf16[16,24,2048]{2,1,0:T(8,128)(2,1)}), bf16[16,24,2048]{2,1,0:T(8,128)(2,1)}, u32[]{:S(2)}, u32[]{:S(2)}) %all-to-all-start.3) | async-done | bytes 1572896 | tf_op jit(solution)/shard_map/all_to_all | solution.py:201
  261.0 1.9 convolution_bitcast_fusion
  262.8 2.9 %fusion.2 = f32[128,2048]{1,0:T(8,128)} fusion(f32[128,2048]{1,0:T(8,128)S(1)} %convolution_bitcast_fusion, bf16[16,24,2048]{2,1,0:T(8,128)(2,1)} %all-to-all-done.3, f32[128,16]{0,1:T(8,128)S(1)} %get-tuple-element.46, s32[128,16]{0,1:T(8,128)S(1)} %get-tuple-element.44), kind=kOutput, calls=%fused_computation.11 | convolution fusion | flops 201785344 | bytes 3686400 | tf_op jit(solution)/shard_map/dot_general | solution.py:235
  265.7 4.4 %fusion.15 = bf16[128,2048]{1,0:T(8,128)(2,1)} fusion(f32[128,2048]{1,0:T(8,128)} %fusion.2, bf16[512,2048]{1,0:T(8,128)(2,1)} %param.47, bf16[128,2048]{1,0:T(8,128)(2,1)S(1)} %get-tuple-element.75, bf16[2048,512]{1,0:T(8,128)(2,1)} %param.46, bf16[128,2048]{1,0:T(8,128)(2,1)} %collective-permute-done.8, f32[128,512]{1,0:T(8,128)S(1)} %fusion.149, ...), kind=kOutput, calls=%fused_computation.28 | convolution fusion | flops 539885568 | bytes 7086592 | tf_op jit(solution)/shard_map/dot_general | solution.py:178
  (183 shorter events, 79.6 us)
Async XLA Ops:
  0.0 186.7 %copy-start = (bf16[1,512,2048]{2,1,0:T(8,128)(2,1)S(1)}, bf16[1,512,2048]{2,1,0:T(8,128)(2,1)}, u32[]{:S(2)}) copy-start(bf16[1,512,2048]{2,1,0:T(8,128)(2,1)} %param.44) | copy-start | bytes 6291460
  0.0 14.0 %copy-start.25 = (bf16[4,256]{1,0:T(4,128)(2,1)S(1)}, bf16[4,256]{1,0:T(4,128)(2,1)}, u32[]{:S(2)}) copy-start(bf16[4,256]{1,0:T(4,128)(2,1)} %param.33) | copy-start | bytes 6148
  0.0 14.7 %copy-start.19 = (s32[128,4]{0,1:T(4,128)S(1)}, s32[128,4]{0,1:T(4,128)}, u32[]{:S(2)}) copy-start(s32[128,4]{0,1:T(4,128)} %param.40) | copy-start | bytes 6148
  3.2 14.0 %collective-permute-start = (bf16[3,1536]{0,1:T(8,128)(2,1)}, bf16[3,1536]{0,1:T(8,128)(2,1)}, u32[]{:S(2)}, u32[]{:S(2)}) collective-permute-start(bf16[3,1536]{0,1:T(8,128)(2,1)} %copy.131), channel_id=1, source_target_pairs={{0,2},{2,4},{4,6},{6,8},{8,10},{10,12},{12,14},{14,16},{16,18},{18... | collective-permute-start | bytes 27656 | tf_op jit(solution)/shard_map/ppermute | solution.py:14
  10.6 7.9 %copy-start.21 = (pred[128]{0:T(512)(128)(4,1)}, pred[128]{0:T(512)(128)(4,1)S(1)}, u32[]{:S(2)}) copy-start(pred[128]{0:T(512)(128)(4,1)S(1)} %get-tuple-element.76) | copy-start | bytes 388
  10.7 7.9 %copy-start.23 = (pred[128]{0:T(512)(128)(4,1)}, pred[128]{0:T(512)(128)(4,1)S(1)}, u32[]{:S(2)}) copy-start(pred[128]{0:T(512)(128)(4,1)S(1)} %get-tuple-element.77) | copy-start | bytes 388
  13.0 5.7 %copy-start.30 = (f32[1,2,8]{2,1,0:T(2,128)}, f32[1,2,8]{2,1,0:T(2,128)S(1)}, u32[]{:S(2)}) copy-start(f32[1,2,8]{2,1,0:T(2,128)S(1)} %get-tuple-element.59) | copy-start | bytes 196
  14.0 4.6 %copy-start.33 = (f32[16]{0:T(128)}, f32[16]{0:T(128)S(1)}, u32[]{:S(2)}) copy-start(f32[16]{0:T(128)S(1)} %exp.109) | copy-start | bytes 196
  27.0 5.7 %copy-start.31 = (pred[128,32]{0,1:T(8,128)(4,1)S(1)}, pred[128,32]{0,1:T(8,128)(4,1)}, u32[]{:S(2)}) copy-start(pred[128,32]{0,1:T(8,128)(4,1)} %fusion.121) | copy-start | bytes 12292
  30.7 9.2 %collective-permute-start.1 = (bf16[1040,128]{1,0:T(8,128)(2,1)}, bf16[1040,128]{1,0:T(8,128)(2,1)}, u32[]{:S(2)}, u32[]{:S(2)}) collective-permute-start(bf16[1040,128]{1,0:T(8,128)(2,1)} %pad_maximum_fusion), channel_id=1, source_target_pairs={{0,2},{2,0},{4,6},{6,4},{8,10},{10,8},{12,14},{14,12},{16,18},{18,... | collective-permute-start | bytes 798728 | tf_op jit(solution)/shard_map/ppermute | solution.py:20
  48.3 9.3 %copy-start.20 = (s32[128,4]{0,1:T(4,128)S(1)}, s32[128,4]{0,1:T(4,128)}, u32[]{:S(2)}) copy-start(s32[128,4]{0,1:T(4,128)} %param.40) | copy-start | bytes 6148
  49.1 11.5 %collective-permute-start.2 = (bf16[1040,128]{1,0:T(8,128)(2,1)}, bf16[1040,128]{1,0:T(8,128)(2,1)}, u32[]{:S(2)}, u32[]{:S(2)}) collective-permute-start(bf16[1040,128]{1,0:T(8,128)(2,1)} %pad_maximum_fusion.1), channel_id=1, source_target_pairs={{0,4},{2,6},{4,0},{6,2},{8,12},{10,14},{12,8},{14,10},{16,20},{18,... | collective-permute-start | bytes 798728 | tf_op jit(solution)/shard_map/ppermute | solution.py:20
  51.9 7.0 %copy-start.14 = (bf16[3,256]{0,1:T(8,128)(2,1)S(1)}, bf16[3,256]{0,1:T(8,128)(2,1)}, u32[]{:S(2)}) copy-start(bf16[3,256]{0,1:T(8,128)(2,1)} %get-tuple-element.38) | copy-start | bytes 4612
  74.1 7.0 %collective-permute-start.3 = (bf16[1040,128]{1,0:T(8,128)(2,1)}, bf16[1040,128]{1,0:T(8,128)(2,1)}, u32[]{:S(2)}, u32[]{:S(2)}) collective-permute-start(bf16[1040,128]{1,0:T(8,128)(2,1)} %pad_maximum_fusion.2), channel_id=1, source_target_pairs={{0,8},{2,10},{4,12},{6,14},{8,0},{10,2},{12,4},{14,6},{16,24},{18,... | collective-permute-start | bytes 798728 | tf_op jit(solution)/shard_map/ppermute | solution.py:20
  77.2 9.6 %copy-start.22 = (pred[128]{0:T(512)(128)(4,1)S(1)}, pred[128]{0:T(512)(128)(4,1)}, u32[]{:S(2)}) copy-start(pred[128]{0:T(512)(128)(4,1)} %copy-done.21) | copy-start | bytes 388
  77.2 9.6 %copy-start.24 = (pred[128]{0:T(512)(128)(4,1)S(1)}, pred[128]{0:T(512)(128)(4,1)}, u32[]{:S(2)}) copy-start(pred[128]{0:T(512)(128)(4,1)} %copy-done.23) | copy-start | bytes 388
  84.6 7.6 %copy-start.13 = (f32[2,2,128,128]{3,2,1,0:T(8,128)S(1)}, f32[2,2,128,128]{3,2,1,0:T(8,128)}, u32[]{:S(2)}) copy-start(f32[2,2,128,128]{3,2,1,0:T(8,128)} %fusion.103) | copy-start | bytes 786436
  87.0 9.7 %copy-start.35 = (f32[16]{0:T(128)S(1)}, f32[16]{0:T(128)}, u32[]{:S(2)}) copy-start(f32[16]{0:T(128)} %get-tuple-element.14) | copy-start | bytes 196
  87.0 9.8 %copy-start.34 = (f32[16]{0:T(128)S(1)}, f32[16]{0:T(128)}, u32[]{:S(2)}) copy-start(f32[16]{0:T(128)} %get-tuple-element.20) | copy-start | bytes 196
  87.0 11.6 %collective-permute-start.4 = (bf16[1040,128]{1,0:T(8,128)(2,1)S(1)}, bf16[1040,128]{1,0:T(8,128)(2,1)}, u32[]{:S(2)}, u32[]{:S(2)}) collective-permute-start(bf16[1040,128]{1,0:T(8,128)(2,1)S(1)} %pad_maximum_fusion.3), channel_id=1, source_target_pairs={{0,16},{2,18},{4,20},{6,22},{8,24},{10,26},{12,28},{14,30},{1,17},... | collective-permute-start | bytes 798728 | tf_op jit(solution)/shard_map/ppermute | solution.py:20
  97.5 3.7 %copy-start.6 = (f32[2,2,8,64,128]{4,3,2,1,0:T(8,128)S(1)}, f32[2,2,8,64,128]{4,3,2,1,0:T(8,128)}, u32[]{:S(2)}) copy-start(f32[2,2,8,64,128]{4,3,2,1,0:T(8,128)} %get-tuple-element.71) | copy-start | bytes 3145732
  97.5 3.7 %copy-start.32 = (f32[2,8]{1,0:T(2,128)S(1)}, f32[2,8]{1,0:T(2,128)}, u32[]{:S(2)}) copy-start(f32[2,8]{1,0:T(2,128)} %fusion.134) | copy-start | bytes 196
  104.2 5.8 %copy-start.12 = (bf16[128,2048]{1,0:T(8,128)(2,1)S(1)}, bf16[128,2048]{1,0:T(8,128)(2,1)}, u32[]{:S(2)}) copy-start(bf16[128,2048]{1,0:T(8,128)(2,1)} %param.24) | copy-start | bytes 1572868
  105.0 5.0 %collective-permute-start.5 = (bf16[128,2048]{1,0:T(8,128)(2,1)S(1)}, bf16[128,2048]{1,0:T(8,128)(2,1)}, u32[]{:S(2)}, u32[]{:S(2)}) collective-permute-start(bf16[128,2048]{1,0:T(8,128)(2,1)S(1)} %convolution_convert_fusion.4), channel_id=1, source_target_pairs={{0,1},{1,0},{2,3},{3,2},{4,5},{5,4},{6,7},{7,6},{8,9},{9,8},{10,11... | collective-permute-start | bytes 1572872 | tf_op jit(solution)/shard_map/ppermute | solution.py:163
  105.1 4.7 %collective-permute-start.7 = (f32[2,128,16]{1,2,0:T(8,128)S(1)}, f32[2,128,16]{1,2,0:T(8,128)S(1)}, u32[]{:S(2)}, u32[]{:S(2)}) collective-permute-start(f32[2,128,16]{1,2,0:T(8,128)S(1)} %get-tuple-element.42), channel_id=1, source_target_pairs={{0,16},{2,18},{4,20},{6,22},{8,24},{10,26},{12,28},{14,30},{16,0},... | collective-permute-start | bytes 49160 | tf_op jit(solution)/shard_map/ppermute | solution.py:20
  110.0 3.3 %copy-start.15 = (f32[2048]{0:T(1024)S(1)}, f32[2048]{0:T(1024)}, u32[]{:S(2)}) copy-start(f32[2048]{0:T(1024)} %param.39) | copy-start | bytes 24580
  115.1 40.5 %all-to-all-start = ((bf16[16,24,2048]{2,1,0:T(8,128)(2,1)}), bf16[16,24,2048]{2,1,0:T(8,128)(2,1)}, u32[]{:S(2)}, u32[]{:S(2)}) async-start(bf16[16,24,2048]{2,1,0:T(8,128)(2,1)} %bitcast.158), calls=%async_computation | async-start | bytes 3145728 | tf_op jit(solution)/shard_map/all_to_all | solution.py:201
  122.4 29.6 %collective-permute-start.6 = (bf16[128,2048]{1,0:T(8,128)(2,1)S(1)}, bf16[128,2048]{1,0:T(8,128)(2,1)}, u32[]{:S(2)}, u32[]{:S(2)}) collective-permute-start(bf16[128,2048]{1,0:T(8,128)(2,1)S(1)} %fusion.40), channel_id=1, source_target_pairs={{0,16},{2,18},{4,20},{6,22},{8,24},{10,26},{12,28},{14,30},{16,0},... | collective-permute-start | bytes 1572872 | tf_op jit(solution)/shard_map/ppermute | solution.py:20
  157.2 27.6 %copy-start.36 = (bf16[1,2048,512]{2,1,0:T(8,128)(2,1)S(1)}, bf16[1,2048,512]{2,1,0:T(8,128)(2,1)}, u32[]{:S(2)}) copy-start(bf16[1,2048,512]{2,1,0:T(8,128)(2,1)} %param.42) | copy-start | bytes 6291460
  191.9 26.9 %all-to-all-start.2 = ((bf16[16,24,2048]{2,1,0:T(8,128)(2,1)}), bf16[16,24,2048]{2,1,0:T(8,128)(2,1)}, u32[]{:S(2)}, u32[]{:S(2)}) async-start(bf16[16,24,2048]{2,1,0:T(8,128)(2,1)} %bitcast.166), calls=%async_computation.2 | async-start | bytes 3145728 | tf_op jit(solution)/shard_map/all_to_all | solution.py:201
  223.4 37.5 %all-to-all-start.3 = ((bf16[16,24,2048]{2,1,0:T(8,128)(2,1)}), bf16[16,24,2048]{2,1,0:T(8,128)(2,1)}, u32[]{:S(2)}, u32[]{:S(2)}) async-start(bf16[16,24,2048]{2,1,0:T(8,128)(2,1)} %bitcast.165), calls=%async_computation.3 | async-start | bytes 3145728 | tf_op jit(solution)/shard_map/all_to_all | solution.py:201
  227.8 37.9 %collective-permute-start.8 = (bf16[128,2048]{1,0:T(8,128)(2,1)}, bf16[128,2048]{1,0:T(8,128)(2,1)}, u32[]{:S(2)}, u32[]{:S(2)}) collective-permute-start(bf16[128,2048]{1,0:T(8,128)(2,1)} %fusion.3), channel_id=1, source_target_pairs={{0,16},{2,18},{4,20},{6,22},{8,24},{10,26},{12,28},{14,30},{16,0},... | collective-permute-start | bytes 1572872 | tf_op jit(solution)/shard_map/ppermute | solution.py:20
  (17 other events, 19.8 us)
where the time goes:
time: 272 us; the launch traced here: 270 us
  waiting for transfers between devices  78.6 us (29%)
  matrix products  46.7 us (17%)
  local copies, waits for them, and re-layouts  45.5 us (17%)
  starting transfers between devices  36.7 us (13%)
  other arithmetic  35.7 us (13%)
  blocking collectives  26.4 us (10%)
    all_to_all x3, waiting for transfers between devices, exchange(): lax.all_to_all(block, ('sp', 'tp'), split_axis=0, concat_axis=0, axis_ind...  46.6 us
    ppermute x7, waiting for transfers between devices, swap(): return lax.ppermute(block, axis, route)  32 us
    all_to_all x1, blocking collectives, exchange(): lax.all_to_all(block, ('sp', 'tp'), split_axis=0, concat_axis=0, axis_ind...  26.4 us
    all_to_all x3, starting transfers between devices, exchange(): lax.all_to_all(block, ('sp', 'tp'), split_axis=0, concat_axis=0, axis_ind...  15.9 us
    ppermute x7, starting transfers between devices, swap(): return lax.ppermute(block, axis, route)  15 us
    dot_general x2, matrix products, expert(): jnp.dot(hidden, routed_down_weight[0], preferred_element_type=jnp.float32)  10.6 us
    unnamed x76, local copies, waits for them, and re-layouts  9.89 us
    another operation x10, other arithmetic  9.68 us
  transfers between devices with their start and end apart: 12, of which 6 were waited for; matrix products, arithmetic and copies ran while one was open for 19% of the time, Pallas kernels for 0%

commit v1 on v0

--- a/solution.py
+++ b/solution.py
@@ -1,6 +1,10 @@
+import functools
+
 import jax
 import jax.numpy as jnp
 from jax import lax
+from jax.experimental import pallas as pl
+from jax.experimental.pallas import tpu as pltpu
 from jax.sharding import PartitionSpec as P
 
 HEAD_DIM = 64
@@ -61,6 +65,550 @@
 def product(spec, *operands):
     return jnp.einsum(
         spec, *[part.astype(jnp.bfloat16) for part in operands], preferred_element_type=jnp.float32
+    )
+
+
+MESH = pl.DeviceIdType.MESH
+PLANES = 4
+COLS = 512
+
+
+def column_chunks(width):
+    step = min(COLS, width)
+    return [(at, step) for at in range(0, width, step)]
+
+
+def pick(values, place, which, index):
+    chosen = jnp.int32(0)
+    for spot, row in enumerate(values):
+        chosen = chosen + (place == spot).astype(jnp.int32) * pick_one(row, which)
+    return chosen
+
+
+def pick_one(row, which):
+    chosen = jnp.int32(0)
+    for spot, value in enumerate(row):
+        chosen = chosen + (which == spot).astype(jnp.int32) * value
+    return chosen
+
+
+def tail_kernel(
+    planes,
+    ring,
+    tp_count,
+    capacity,
+    fanout,
+    mixed_ref,
+    stream_ref,
+    gain_ref,
+    table_ref,
+    out_weight_hbm,
+    gate_hbm,
+    up_hbm,
+    down_hbm,
+    common_gate_hbm,
+    common_up_hbm,
+    common_down_hbm,
+    out_ref,
+    out_weight,
+    gate,
+    up,
+    down,
+    common_gate,
+    common_up,
+    common_down,
+    tables,
+    total,
+    residual,
+    part_out,
+    part_in,
+    rows,
+    sent,
+    arrived,
+    flat,
+    hidden,
+    answer,
+    returned,
+    sums_out,
+    sums_in,
+    weight_sem,
+    part_send,
+    part_recv,
+    table_send,
+    table_recv,
+    rows_up,
+    rows_down,
+    rows_recv,
+    go_send,
+    go_recv,
+    back_send,
+    back_recv,
+    sums_send,
+    sums_recv,
+):
+    chip = lax.axis_index("sp")
+    core = lax.axis_index("tp")
+    chips = ring // tp_count
+    plane = chip // chips
+    mine = (chip % chips) * tp_count + core
+    count, width = rows.shape[1], rows.shape[2]
+    order = [sorted(range(planes), key=lambda s: (abs(s - z), s)) for z in range(planes)]
+
+    def in_plane(spot):
+        return (plane * chips + spot // tp_count, spot % tp_count)
+
+    def in_line(spot):
+        return (spot * chips + chip % chips, core)
+
+    loads = [
+        pltpu.make_async_copy(source, target, weight_sem.at[number])
+        for number, (source, target) in enumerate(
+            [
+                (out_weight_hbm, out_weight),
+                (common_gate_hbm, common_gate),
+                (common_up_hbm, common_up),
+                (common_down_hbm, common_down),
+                (gate_hbm.at[0], gate),
+                (up_hbm.at[0], up),
+                (down_hbm.at[0], down),
+            ]
+        )
+    ]
+    for load in loads:
+        load.start()
+
+    barrier = pltpu.get_barrier_semaphore()
+    for ahead in range(1, ring):
+        pl.semaphore_signal(
+            barrier, inc=1, device_id=in_plane((mine + ahead) % ring), device_id_type=MESH
+        )
+    for ahead in range(1, planes):
+        pl.semaphore_signal(
+            barrier, inc=1, device_id=in_line((plane + ahead) % planes), device_id_type=MESH
+        )
+    pl.semaphore_wait(barrier, ring + planes - 2)
+
+    def table_copy(ahead, owner):
+        return pltpu.make_async_remote_copy(
+            src_ref=table_ref,
+            dst_ref=tables.at[owner],
+            send_sem=table_send.at[ahead],
+            recv_sem=table_recv.at[owner],
+            device_id=in_line((plane + ahead) % planes),
+            device_id_type=MESH,
+        )
+
+    for ahead in range(1, planes):
+        table_copy(ahead, plane).start()
+    tables[plane] = table_ref[...]
+
+    def part_copy(ahead):
+        return pltpu.make_async_remote_copy(
+            src_ref=part_out.at[ahead - 1],
+            dst_ref=part_in.at[ahead - 1],
+            send_sem=part_send.at[ahead - 1],
+            recv_sem=part_recv.at[ahead - 1],
+            device_id=(chip, (core + ahead) % tp_count),
+            device_id_type=MESH,
+        )
+
+    loads[0].wait()
+    for ahead in range(1, tp_count):
+        owner = (core + ahead) % tp_count
+        held = mixed_ref[pl.ds(pl.multiple_of(owner * count, count), count), :]
+        for at, step in column_chunks(width):
+            part_out[ahead - 1, :, at : at + step] = jnp.dot(
+                held, out_weight[:, at : at + step], preferred_element_type=jnp.float32
+            ).astype(jnp.bfloat16)
+        part_copy(ahead).start()
+    held = mixed_ref[pl.ds(pl.multiple_of(core * count, count), count), :]
+    for at, step in column_chunks(width):
+        total[:, at : at + step] = stream_ref[:, at : at + step].astype(jnp.float32) + jnp.dot(
+            held, out_weight[:, at : at + step], preferred_element_type=jnp.float32
+        )
+    for ahead in range(1, tp_count):
+        part_copy(ahead).wait_recv()
+    band = 16
+
+    def norm_band(number, carry):
+        spot = pl.ds(pl.multiple_of(number * band, band), band)
+        summed = total[spot, :]
+        for ahead in range(1, tp_count):
+            summed = summed + part_in[ahead - 1, spot, :].astype(jnp.float32)
+        rounded = summed.astype(jnp.bfloat16)
+        wide = rounded.astype(jnp.float32)
+        total[spot, :] = wide
+        scale = lax.rsqrt(jnp.mean(wide * wide, axis=-1, keepdims=True) + 1e-06)
+        rows[plane, spot, :] = (wide * scale * gain_ref[...]).astype(jnp.bfloat16)
+        return carry
+
+    lax.fori_loop(0, count // band, norm_band, 0)
+
+    def rows_copy(owner, target, sem):
+        return pltpu.make_async_remote_copy(
+            src_ref=rows.at[owner],
+            dst_ref=rows.at[owner],
+            send_sem=sem.at[owner],
+            recv_sem=rows_recv.at[owner],
+            device_id=in_line(target),
+            device_id_type=MESH,
+        )
+
+    def go_copy(owner, ahead):
+        spot = (mine + ahead) % ring
+        return pltpu.make_async_remote_copy(
+            src_ref=sent.at[owner, spot],
+            dst_ref=arrived.at[owner, mine],
+            send_sem=go_send.at[owner, spot],
+            recv_sem=go_recv.at[owner, mine],
+            device_id=in_plane(spot),
+            device_id_type=MESH,
+        )
+
+    def go_wait(owner, ahead):
+        spot = (mine + ahead) % ring
+        return pltpu.make_async_remote_copy(
+            src_ref=sent.at[owner, spot],
+            dst_ref=arrived.at[owner, spot],
+            send_sem=go_send.at[owner, spot],
+            recv_sem=go_recv.at[owner, spot],
+            device_id=in_plane(spot),
+            device_id_type=MESH,
+        )
+
+    def back_copy(owner, ahead):
+        spot = (mine + ahead) % ring
+        return pltpu.make_async_remote_copy(
+            src_ref=answer.at[owner, spot],
+            dst_ref=returned.at[owner, mine],
+            send_sem=back_send.at[owner, spot],
+            recv_sem=back_recv.at[owner, mine],
+            device_id=in_plane(spot),
+            device_id_type=MESH,
+        )
+
+    def back_wait(owner, ahead):
+        spot = (mine + ahead) % ring
+        return pltpu.make_async_remote_copy(
+            src_ref=answer.at[owner, spot],
+            dst_ref=returned.at[owner, spot],
+            send_sem=back_send.at[owner, spot],
+            recv_sem=back_recv.at[owner, spot],
+            device_id=in_plane(spot),
+            device_id_type=MESH,
+        )
+
+    def sums_copy(owner):
+        return pltpu.make_async_remote_copy(
+            src_ref=sums_out.at[owner],
+            dst_ref=sums_in.at[plane],
+            send_sem=sums_send.at[owner],
+            recv_sem=sums_recv.at[plane],
+            device_id=in_line(owner),
+            device_id_type=MESH,
+        )
+
+    def sums_wait(owner):
+        return pltpu.make_async_remote_copy(
+            src_ref=sums_out.at[owner],
+            dst_ref=sums_in.at[owner],
+            send_sem=sums_send.at[owner],
+            recv_sem=sums_recv.at[owner],
+            device_id=in_line(owner),
+            device_id_type=MESH,
+        )
+
+    def slots_of(owner):
+        table = tables[owner]
+        first = (plane * ring).astype(jnp.float32)
+        names = lax.broadcasted_iota(jnp.int32, (ring, count), 0).astype(jnp.float32) + first
+        hits = jnp.zeros((ring, count), jnp.float32)
+        share = jnp.zeros((ring, count), jnp.float32)
+        for turn in range(fanout):
+            named = table[turn : turn + 1, :] == names
+            hits = hits + jnp.where(named, 1.0, 0.0)
+            share = share + jnp.where(named, table[fanout + turn : fanout + turn + 1, :], 0.0)
+        before = lax.broadcasted_iota(jnp.int32, (count, count), 0)
+        after = lax.broadcasted_iota(jnp.int32, (count, count), 1)
+        earlier = jnp.where(before < after, 1.0, 0.0).astype(jnp.bfloat16)
+        slot = jnp.dot(hits.astype(jnp.bfloat16), earlier, preferred_element_type=jnp.float32)
+        return jnp.where(hits > 0.5, slot, -1.0), share
+
+    places = lax.broadcasted_iota(jnp.int32, (capacity, count), 0).astype(jnp.float32)
+
+    def wait_table(owner):
+        ahead = (owner + planes - plane) % planes
+        table_copy(ahead, owner).wait_recv()
+
+    def dispatch(owner):
+        @pl.when(owner != plane)
+        def _():
+            rows_copy(owner, owner, rows_up).wait_recv()
+            wait_table(owner)
+
+        @pl.when((owner <= plane) & (plane < planes - 1))
+        def _():
+            rows_copy(owner, plane + 1, rows_up).start()
+
+        @pl.when((owner >= plane) & (plane > 0))
+        def _():
+            rows_copy(owner, plane - 1, rows_down).start()
+
+        slot, _ = slots_of(owner)
+        chosen = jnp.concatenate(
+            [
+                jnp.where(slot[spot : spot + 1, :] == places, 1.0, 0.0)
+                for spot in range(ring)
+            ],
+            axis=0,
+        ).astype(jnp.bfloat16)
+        for at, step in column_chunks(width):
+            picked = jnp.dot(
+                chosen, rows[owner, :, at : at + step], preferred_element_type=jnp.float32
+            )
+            for spot in range(ring):
+                sent[owner, spot, :, at : at + step] = picked[
+                    spot * capacity : (spot + 1) * capacity
+                ].astype(jnp.bfloat16)
+        for ahead in range(1, ring):
+            go_copy(owner, ahead).start()
+        arrived[owner, mine] = sent[owner, mine]
+
+    def ffn(x_ref, gate_ref, up_ref, down_ref, hidden_ref, put):
+        for at, step in column_chunks(gate_ref.shape[1]):
+            half = step // 2
+            for lane in (at, at + half):
+                g = jnp.dot(
+                    x_ref[...], gate_ref[:, lane : lane + half], preferred_element_type=jnp.float32
+                )
+                u = jnp.dot(
+                    x_ref[...], up_ref[:, lane : lane + half], preferred_element_type=jnp.float32
+                )
+                hidden_ref[:, lane : lane + half] = (jax.nn.silu(g) * u).astype(jnp.bfloat16)
+        for at, step in column_chunks(width):
+            put(
+                at,
+                step,
+                jnp.dot(
+                    hidden_ref[...],
+                    down_ref[:, at : at + step],
+                    preferred_element_type=jnp.float32,
+                ),
+            )
+
+    def serve(owner):
+        for ahead in range(1, ring):
+            go_wait(owner, ahead).wait_recv()
+        for at, step in column_chunks(width):
+            flat[:, at : at + step] = jnp.concatenate(
+                [
+                    arrived[owner, spot, :, at : at + step].astype(jnp.float32)
+                    for spot in range(ring)
+                ],
+                axis=0,
+            ).astype(jnp.bfloat16)
+
+        def put(at, step, value):
+            for spot in range(ring):
+                answer[owner, spot, :, at : at + step] = value[
+                    spot * capacity : (spot + 1) * capacity
+                ].astype(jnp.bfloat16)
+
+        ffn(flat, gate, up, down, hidden, put)
+        for ahead in range(1, ring):
+            back_copy(owner, ahead).start()
+        returned[owner, mine] = answer[owner, mine]
+
+    def collect(owner):
+        for ahead in range(1, ring):
+            back_wait(owner, ahead).wait_recv()
+        slot, share = slots_of(owner)
+        spread = jnp.concatenate(
+            [
+                jnp.where(slot[spot : spot + 1, :] == places, share[spot : spot + 1, :], 0.0)
+                for spot in range(ring)
+            ],
+            axis=0,
+        )
+        coarse = spread.astype(jnp.bfloat16)
+        fine = (spread - coarse.astype(jnp.float32)).astype(jnp.bfloat16)
+        contract = (((0,), (0,)), ((), ()))
+        for at, step in column_chunks(width):
+            back = jnp.concatenate(
+                [
+                    returned[owner, spot, :, at : at + step].astype(jnp.float32)
+                    for spot in range(ring)
+                ],
+                axis=0,
+            ).astype(jnp.bfloat16)
+            value = lax.dot_general(coarse, back, contract, preferred_element_type=jnp.float32)
+            value = value + lax.dot_general(
+                fine, back, contract, preferred_element_type=jnp.float32
+            )
+
+            @pl.when(owner == plane)
+            def _():
+                total[:, at : at + step] += value
+
+            @pl.when(owner != plane)
+            def _():
+                sums_out[owner, :, at : at + step] = value.astype(jnp.bfloat16)
+
+        @pl.when(owner != plane)
+        def _():
+            sums_copy(owner).start()
+
+    def source(turn):
+        return pick(order, plane, turn, 0)
+
+    def step(turn, carry):
+        @pl.when(turn < planes)
+        def _():
+            dispatch(source(turn))
+
+        @pl.when(turn == 0)
+        def _():
+            for load in loads[1:]:
+                load.wait()
+
+            def put(at, step, value):
+                total[:, at : at + step] += value
+
+            ffn(rows.at[plane], common_gate, common_up, common_down, residual, put)
+
+        @pl.when((turn >= 1) & (turn <= planes))
+        def _():
+            serve(source(turn - 1))
+
+        @pl.when(turn >= 2)
+        def _():
+            collect(source(turn - 2))
+
+        return carry
+
+    lax.fori_loop(0, planes + 2, step, 0)
+
+    for ahead in range(1, planes):
+        sums_wait((plane + ahead) % planes).wait_recv()
+
+    def last_band(number, carry):
+        spot = pl.ds(pl.multiple_of(number * band, band), band)
+        summed = total[spot, :]
+        for ahead in range(1, planes):
+            summed = summed + sums_in[(plane + ahead) % planes, spot, :].astype(jnp.float32)
+        out_ref[spot, :] = summed.astype(jnp.bfloat16)
+        return carry
+
+    lax.fori_loop(0, count // band, last_band, 0)
+
+    for ahead in range(1, tp_count):
+        part_copy(ahead).wait_send()
+    for ahead in range(1, planes):
+        table_copy(ahead, plane).wait_send()
+        sums_copy((plane + ahead) % planes).wait_send()
+    for owner in range(planes):
+
+        @pl.when((owner <= plane) & (plane < planes - 1))
+        def _():
+            rows_copy(owner, plane + 1, rows_up).wait_send()
+
+        @pl.when((owner >= plane) & (plane > 0))
+        def _():
+            rows_copy(owner, plane - 1, rows_down).wait_send()
+
+    def drain(owner, carry):
+        for ahead in range(1, ring):
+            go_copy(owner, ahead).wait_send()
+            back_copy(owner, ahead).wait_send()
+        return carry
+
+    lax.fori_loop(0, planes, drain, 0)
+
+
+def tail(
+    mixed,
+    stream,
+    gain,
+    index,
+    weight,
+    out_weight,
+    gate,
+    up,
+    down,
+    common_gate,
+    common_up,
+    common_down,
+):
+    sp_count, tp_count = lax.axis_size("sp"), lax.axis_size("tp")
+    planes = PLANES if sp_count % PLANES == 0 else 1
+    ring = sp_count // planes * tp_count
+    count, width = stream.shape
+    fanout = index.shape[1]
+    experts = sp_count * tp_count
+    capacity = max(2, (3 * count * fanout + 2 * experts - 1) // (2 * experts))
+    capacity = (capacity + 7) // 8 * 8
+    table = jnp.concatenate([index.astype(jnp.float32).T, weight.T], axis=0)
+    bf16 = jnp.bfloat16
+    vmem, anywhere = pl.BlockSpec(memory_space=pltpu.VMEM), pl.BlockSpec(memory_space=pl.ANY)
+    slots = (planes, ring, capacity, width)
+    dma = pltpu.SemaphoreType.DMA
+    return pl.pallas_call(
+        functools.partial(tail_kernel, planes, ring, tp_count, capacity, fanout),
+        out_shape=jax.ShapeDtypeStruct((count, width), bf16),
+        in_specs=[vmem] * 4 + [anywhere] * 7,
+        out_specs=vmem,
+        scratch_shapes=[
+            pltpu.VMEM(out_weight.shape, bf16),
+            pltpu.VMEM(gate.shape[1:], bf16),
+            pltpu.VMEM(up.shape[1:], bf16),
+            pltpu.VMEM(down.shape[1:], bf16),
+            pltpu.VMEM(common_gate.shape, bf16),
+            pltpu.VMEM(common_up.shape, bf16),
+            pltpu.VMEM(common_down.shape, bf16),
+            pltpu.VMEM((planes, 2 * fanout, count), jnp.float32),
+            pltpu.VMEM((count, width), jnp.float32),
+            pltpu.VMEM((count, common_gate.shape[1]), bf16),
+            pltpu.VMEM((tp_count - 1, count, width), bf16),
+            pltpu.VMEM((tp_count - 1, count, width), bf16),
+            pltpu.VMEM((planes, count, width), bf16),
+            pltpu.VMEM(slots, bf16),
+            pltpu.VMEM(slots, bf16),
+            pltpu.VMEM((ring * capacity, width), bf16),
+            pltpu.VMEM((ring * capacity, gate.shape[2]), bf16),
+            pltpu.VMEM(slots, bf16),
+            pltpu.VMEM(slots, bf16),
+            pltpu.VMEM((planes, count, width), bf16),
+            pltpu.VMEM((planes, count, width), bf16),
+            dma((7,)),
+            dma((tp_count - 1,)),
+            dma((tp_count - 1,)),
+            dma((planes,)),
+            dma((planes,)),
+            dma((planes,)),
+            dma((planes,)),
+            dma((planes,)),
+            dma((planes, ring)),
+            dma((planes, ring)),
+            dma((planes, ring)),
+            dma((planes, ring)),
+            dma((planes,)),
+            dma((planes,)),
+        ],
+        compiler_params=pltpu.CompilerParams(
+            collective_id=0, has_side_effects=True, vmem_limit_bytes=60 * 2**20
+        ),
+    )(
+        mixed,
+        stream,
+        gain.reshape(1, -1),
+        table,
+        out_weight,
+        gate,
+        up,
+        down,
+        common_gate,
+        common_up,
+        common_down,
     )
 
 
@@ -148,105 +696,20 @@
     ).reshape(length, groups, per_group * HEAD_DIM)
     norm_scale = lax.rsqrt(jnp.mean(gated * gated, axis=-1, keepdims=True) + 1e-06)
     mixer_out = ((gated * norm_scale).reshape(length, -1) * grouped_norm_gain).astype(jnp.bfloat16)
-    row_count = stream.shape[0]
-    tp_count = lax.axis_size("tp")
-    core = lax.axis_index("tp")
-
-    def share_of(owner):
-        rows = lax.dynamic_slice_in_dim(mixer_out, owner * row_count, row_count, 0)
-        return jnp.dot(rows, mixer_output_weight, preferred_element_type=jnp.float32)
-
-    shares = []
-    for ahead in range(1, tp_count):
-        route = [(i, (i + ahead) % tp_count) for i in range(tp_count)]
-        part = share_of((core + ahead) % tp_count).astype(jnp.bfloat16)
-        shares.append(lax.ppermute(part, "tp", route))
-    summed = share_of(core)
-    for part in shares:
-        summed = summed + part.astype(jnp.float32)
-    residual = (stream.astype(jnp.float32) + summed).astype(jnp.bfloat16)
-    widened = residual.astype(jnp.float32)
-    normed = (
-        widened
-        * lax.rsqrt(jnp.mean(widened * widened, axis=-1, keepdims=True) + 1e-06)
-        * expert_norm_gain
-    ).astype(jnp.bfloat16)
-    shared_hidden = (
-        jax.nn.silu(jnp.dot(normed, common_gate_weight, preferred_element_type=jnp.float32))
-        * jnp.dot(normed, common_up_weight, preferred_element_type=jnp.float32)
-    ).astype(jnp.bfloat16)
-    shared = jnp.dot(shared_hidden, common_down_weight, preferred_element_type=jnp.float32)
-    sp_count = lax.axis_size("sp")
-    experts = sp_count * tp_count
-    fanout = chosen_expert_index.shape[1]
-    capacity = max(2, (3 * row_count * fanout + 2 * experts - 1) // (2 * experts))
-    named = chosen_expert_index[:, :, None] == jnp.arange(experts, dtype=jnp.int32)
-    hits = jnp.any(named, axis=1)
-    share = jnp.sum(jnp.where(named, chosen_expert_weight[:, :, None], 0.0), axis=1)
-    ahead = (jnp.arange(row_count)[:, None] > jnp.arange(row_count)[None, :]).astype(jnp.bfloat16)
-    slot = jnp.dot(ahead, hits.astype(jnp.bfloat16), preferred_element_type=jnp.float32)
-    slot = jnp.where(hits, slot.astype(jnp.int32), -1)
-    places = jnp.arange(capacity, dtype=jnp.int32)
-    half = experts // 2
-    side = lax.axis_index("sp") // (sp_count // 2)
-    sides = [list(range(half)), list(range(half, experts))]
-    across = sp_count // 2
-    tables = jnp.stack([slot.astype(jnp.float32), share])
-    near_table = lax.dynamic_slice_in_dim(tables, side * half, half, 2)
-    far_table = swap(
-        lax.dynamic_slice_in_dim(tables, (1 - side) * half, half, 2), "sp", across, False
-    )
-
-    def exchange(block):
-        return lax.all_to_all(
-            block,
-            ("sp", "tp"),
-            split_axis=0,
-            concat_axis=0,
-            axis_index_groups=sides,
-            tiled=True,
-        )
-
-    def dispatch(table, rows):
-        slots = table[0].astype(jnp.int32)
-        pick = slots.T[:, None, :] == places[None, :, None]
-        pick = pick.reshape(half * capacity, row_count).astype(jnp.bfloat16)
-        picked = jnp.dot(pick, rows, preferred_element_type=jnp.float32)
-        return exchange(picked.astype(jnp.bfloat16).reshape(half, capacity, -1))
-
-    def expert(arrived):
-        flat_rows = arrived.reshape(half * capacity, -1)
-        hidden = (
-            jax.nn.silu(
-                jnp.dot(flat_rows, routed_gate_weight[0], preferred_element_type=jnp.float32)
-            )
-            * jnp.dot(flat_rows, routed_up_weight[0], preferred_element_type=jnp.float32)
-        ).astype(jnp.bfloat16)
-        result = jnp.dot(hidden, routed_down_weight[0], preferred_element_type=jnp.float32)
-        return result.astype(jnp.bfloat16).reshape(arrived.shape)
-
-    def collect(table, returned):
-        slots = table[0].astype(jnp.int32)
-        spread = jnp.where(slots[:, :, None] == places, table[1][:, :, None], 0.0)
-        spread = spread.reshape(row_count, half * capacity)
-        coarse = lax.reduce_precision(spread, 8, 7)
-        fine = (spread - coarse).astype(jnp.bfloat16)
-        back = returned.reshape(half * capacity, -1)
-        return jnp.dot(
-            coarse.astype(jnp.bfloat16), back, preferred_element_type=jnp.float32
-        ) + jnp.dot(fine, back, preferred_element_type=jnp.float32)
-
-    far_rows = swap(normed, "sp", across, False)
-    near_rows = dispatch(near_table, normed)
-    near_rows, far_rows = lax.optimization_barrier((near_rows, far_rows))
-    far_arrived = dispatch(far_table, far_rows)
-    near_out = expert(near_rows)
-    far_out = expert(far_arrived)
-    far_sum = collect(far_table, exchange(far_out)).astype(jnp.bfloat16)
-    near_out, far_sum = lax.optimization_barrier((near_out, far_sum))
-    from_far = swap(far_sum, "sp", across, False)
-    near_sum = collect(near_table, exchange(near_out))
-    return (widened + shared + near_sum + from_far.astype(jnp.float32)).astype(jnp.bfloat16)
+    return tail(
+        mixer_out,
+        stream,
+        expert_norm_gain,
+        chosen_expert_index,
+        chosen_expert_weight,
+        mixer_output_weight,
+        routed_gate_weight,
+        routed_up_weight,
+        routed_down_weight,
+        common_gate_weight,
+        common_up_weight,
+        common_down_weight,
+    )
 
 
 def solution(mesh):

time: 272 us -> 200 us (0.74)
  the two profiles are of different devices: /device:TPU:0 before, /device:TPU:25 now
where the time goes in v1:
time: 200 us; the launch traced here: 199 us
  Pallas kernels  123 us (62%)
  local copies, waits for them, and re-layouts  23.3 us (12%)
  waiting for transfers between devices  20.3 us (10%)
  other arithmetic  19.4 us (10%)
  starting transfers between devices  7.33 us (4%)
  matrix products  5.66 us (3%)
    pallas_call x1, Pallas kernels, tail(): pl.pallas_call(functools.partial(tail_kernel, planes, ring, tp_count, cap...  123 us
    ppermute x4, waiting for transfers between devices, swap(): return lax.ppermute(block, axis, route)  20.3 us
    dot_general x4, matrix products, product(): jnp.einsum(spec, *[part.astype(jnp.bfloat16) for part in operands], prefe...  5.66 us
    another operation x10, other arithmetic  4.94 us
    ppermute x4, starting transfers between devices, swap(): return lax.ppermute(block, axis, route)  4.21 us
  transfers between devices with their start and end apart: 5, of which 3 were waited for; matrix products, arithmetic and copies ran while one was open for 10% of the time, Pallas kernels for 0%

profile of v1, /device:TPU:25, one launch (start us, length us, event | category | flops | bytes accessed | tf_op | source)
XLA Modules:
  0.0 199.5 jit_solution(15442646781479213318)
XLA Ops:
  2.2 3.1 %collective-permute-start = (bf16[3,1536]{1,0:T(4,128)(2,1)S(1)}, bf16[3,1536]{1,0:T(4,128)(2,1)S(1)}, u32[]{:S(2)}, u32[]{:S(2)}) collective-permute-start(bf16[3,1536]{1,0:T(4,128)(2,1)S(1)} %pad_maximum_fusion.4), channel_id=1, source_target_pairs={{0,2},{2,4},{4,6},{6,8},{8,10},{10,12},{12,14},{14,16},{16,18},{18... | collective-permute-start | bytes 27656 | tf_op jit(solution)/shard_map/ppermute | solution.py:18
  5.3 1.5 fusion.36
  7.1 0.8 fusion.56
  7.9 0.9 fusion.54
  8.8 1.0 fusion.52
  9.9 1.3 convert_bitcast_fusion
  14.3 0.8 copy.118
  15.1 2.1 %multiply_reduce_fusion.1 = (f32[2,8,64,128]{3,2,1,0:T(8,128)S(1)}, f32[2,2,8,64,128]{4,3,2,1,0:T(8,128)}) fusion(f32[2,2,8]{2,1,0:T(2,128)S(1)} %subtract_exponential_fusion.1, bf16[2,128,2,128,1]{3,2,1,0,4:T(2,128)(2,1)S(1)} %bitcast.69, f32[2,128,2,8,64]{1,4,3,2,0:T(8,128)S(1)} %copy.118, f32[2,128,2,8]{1,3,2,0:T(8,128)} %copy.124, ...), kind=kOutput, calls=%fused_computation.20 | convolution fusion | flops 68288512 | bytes 2785408 | tf_op jit(solution)/shard_map/bsgn,bsgep->bgepn/dot_general | solution.py:66
  17.3 1.3 collective-permute-start.1
  19.4 1.3 convert_multiply_fusion
  20.7 3.7 %collective-permute-done.1 = bf16[1040,128]{1,0:T(8,128)(2,1)} collective-permute-done((bf16[1040,128]{1,0:T(8,128)(2,1)S(1)}, bf16[1040,128]{1,0:T(8,128)(2,1)}, u32[]{:S(2)}, u32[]{:S(2)}) %collective-permute-start.1) | collective-permute-done | bytes 266272 | tf_op jit(solution)/shard_map/ppermute | solution.py:24
  24.4 1.0 convert_element_type.82
  26.6 1.2 fusion.49
  28.5 1.2 collective-permute-start.2
  31.8 1.7 reshape.367
  33.5 1.8 copy.133
  36.0 0.8 fusion.55
  36.9 1.0 convert_element_type.83
  39.0 0.8 reduce-precision_reduce_fusion.1
  40.6 1.4 fusion.44
  42.9 5.1 %collective-permute-done.3 = bf16[1040,128]{1,0:T(8,128)(2,1)S(1)} collective-permute-done((bf16[1040,128]{1,0:T(8,128)(2,1)S(1)}, bf16[1040,128]{1,0:T(8,128)(2,1)S(1)}, u32[]{:S(2)}, u32[]{:S(2)}) %collective-permute-start.3) | collective-permute-done | bytes 266272 | tf_op jit(solution)/shard_map/ppermute | solution.py:24
  48.5 0.8 select_convert_fusion
  49.4 1.5 collective-permute-start.4
  50.9 1.9 convolution_bitcast_fusion.1
  52.9 1.0 slice.211
  54.2 11.5 %collective-permute-done.4 = bf16[1040,128]{1,0:T(8,128)(2,1)} collective-permute-done((bf16[1040,128]{1,0:T(8,128)(2,1)S(1)}, bf16[1040,128]{1,0:T(8,128)(2,1)}, u32[]{:S(2)}, u32[]{:S(2)}) %collective-permute-start.4) | collective-permute-done | bytes 266272 | tf_op jit(solution)/shard_map/ppermute | solution.py:24
  65.7 1.0 slice.217
  68.2 1.4 multiply_reduce_fusion
  69.6 2.2 %copy.141 = f32[2,128,2,8,64]{4,3,2,1,0:T(8,128)S(1)} copy(f32[2,128,2,8,64]{1,4,3,2,0:T(8,128)} %get-tuple-element.55) | data formatting | bytes 2097152 | tf_op jit(solution)/shard_map/reshape | solution.py:694
  73.4 1.2 multiply_convert_fusion.2.mixed_ref
  74.6 123.0 %shard_map.226 = bf16[128,2048]{1,0:T(8,128)(2,1)} custom-call(bf16[256,1024]{1,0:T(8,128)(2,1)} %multiply_convert_fusion.2.mixed_ref, bf16[128,2048]{1,0:T(8,128)(2,1)} %stream_ref.1, f32[1,2048]{1,0:T(1,128)} %bitcast.76, f32[8,128]{1,0:T(8,128)} %pad_maximum_fusion.5.table_ref, bf16[1024,2048]{1,0:T(8,128)(2,1)} %out_weight_hbm.1, ...), custom_call_target="tpu_custom_call" | custom-call | tf_op jit(solution)/shard_map/pallas_call | solution.py:555
  197.6 1.9 copy.167
  (137 shorter events, 17.7 us)
Async XLA Ops:
  0.0 12.6 %copy-start.12 = (bf16[256,256]{1,0:T(8,128)(2,1)S(1)}, bf16[256,256]{1,0:T(8,128)(2,1)}, u32[]{:S(2)}) copy-start(bf16[256,256]{1,0:T(8,128)(2,1)} %param.26) | copy-start | bytes 393220
  0.0 12.6 %copy-start.11 = (bf16[256,256]{1,0:T(8,128)(2,1)S(1)}, bf16[256,256]{1,0:T(8,128)(2,1)}, u32[]{:S(2)}) copy-start(bf16[256,256]{1,0:T(8,128)(2,1)} %param.27) | copy-start | bytes 393220
  2.2 10.4 %collective-permute-start = (bf16[3,1536]{1,0:T(4,128)(2,1)S(1)}, bf16[3,1536]{1,0:T(4,128)(2,1)S(1)}, u32[]{:S(2)}, u32[]{:S(2)}) collective-permute-start(bf16[3,1536]{1,0:T(4,128)(2,1)S(1)} %pad_maximum_fusion.4), channel_id=1, source_target_pairs={{0,2},{2,4},{4,6},{6,8},{8,10},{10,12},{12,14},{14,16},{16,18},{18... | collective-permute-start | bytes 27656 | tf_op jit(solution)/shard_map/ppermute | solution.py:18
  6.8 6.2 %copy-start.10 = (bf16[256,1024]{1,0:T(8,128)(2,1)S(1)}, bf16[256,1024]{1,0:T(8,128)(2,1)}, u32[]{:S(2)}) copy-start(bf16[256,1024]{1,0:T(8,128)(2,1)} %param.25) | copy-start | bytes 1572868
  7.0 5.5 %copy-start.2 = (f32[2,128,2,8]{3,2,1,0:T(2,128)}, f32[2,128,2,8]{3,2,1,0:T(2,128)S(1)}, u32[]{:S(2)}) copy-start(f32[2,128,2,8]{3,2,1,0:T(2,128)S(1)} %fusion.58) | copy-start | bytes 49156
  7.1 5.5 %copy-start.17 = (pred[128]{0:T(512)(128)(4,1)}, pred[128]{0:T(512)(128)(4,1)S(1)}, u32[]{:S(2)}) copy-start(pred[128]{0:T(512)(128)(4,1)S(1)} %get-tuple-element.58) | copy-start | bytes 388
  7.1 5.5 %copy-start.20 = (pred[128]{0:T(512)(128)(4,1)}, pred[128]{0:T(512)(128)(4,1)S(1)}, u32[]{:S(2)}) copy-start(pred[128]{0:T(512)(128)(4,1)S(1)} %get-tuple-element.59) | copy-start | bytes 388
  8.8 3.8 %copy-start.26 = (f32[1,2,8]{2,1,0:T(2,128)}, f32[1,2,8]{2,1,0:T(2,128)S(1)}, u32[]{:S(2)}) copy-start(f32[1,2,8]{2,1,0:T(2,128)S(1)} %get-tuple-element.41) | copy-start | bytes 196
  9.9 2.7 %copy-start.29 = (f32[16]{0:T(128)}, f32[16]{0:T(128)S(1)}, u32[]{:S(2)}) copy-start(f32[16]{0:T(128)S(1)} %exp.98) | copy-start | bytes 196
  15.1 4.1 %copy-start.27 = (f32[1,2,8]{2,1,0:T(2,128)S(1)}, f32[1,2,8]{2,1,0:T(2,128)}, u32[]{:S(2)}) copy-start(f32[1,2,8]{2,1,0:T(2,128)} %copy-done.26) | copy-start | bytes 196
  15.1 4.2 %copy-start.30 = (f32[16]{0:T(128)S(1)}, f32[16]{0:T(128)}, u32[]{:S(2)}) copy-start(f32[16]{0:T(128)} %copy-done.29) | copy-start | bytes 196
  15.1 4.3 %copy-start.5 = (bf16[256,1024]{1,0:T(8,128)(2,1)S(1)}, bf16[256,1024]{1,0:T(8,128)(2,1)}, u32[]{:S(2)}) copy-start(bf16[256,1024]{1,0:T(8,128)(2,1)} %param.28) | copy-start | bytes 1572868
  17.2 9.3 %copy-start.18 = (pred[128]{0:T(512)(128)(4,1)S(1)}, pred[128]{0:T(512)(128)(4,1)}, u32[]{:S(2)}) copy-start(pred[128]{0:T(512)(128)(4,1)} %copy-done.17) | copy-start | bytes 388
  17.2 9.3 %copy-start.21 = (pred[128]{0:T(512)(128)(4,1)S(1)}, pred[128]{0:T(512)(128)(4,1)}, u32[]{:S(2)}) copy-start(pred[128]{0:T(512)(128)(4,1)} %copy-done.20) | copy-start | bytes 388
  17.3 7.2 %collective-permute-start.1 = (bf16[1040,128]{1,0:T(8,128)(2,1)S(1)}, bf16[1040,128]{1,0:T(8,128)(2,1)}, u32[]{:S(2)}, u32[]{:S(2)}) collective-permute-start(bf16[1040,128]{1,0:T(8,128)(2,1)S(1)} %pad_maximum_fusion), channel_id=1, source_target_pairs={{0,2},{2,0},{4,6},{6,4},{8,10},{10,8},{12,14},{14,12},{16,18},{18,... | collective-permute-start | bytes 798728 | tf_op jit(solution)/shard_map/ppermute | solution.py:24
  20.7 9.1 %copy-start.23 = (f32[4,128]{1,0:T(4,128)S(1)}, f32[4,128]{1,0:T(4,128)}, u32[]{:S(2)}) copy-start(f32[4,128]{1,0:T(4,128)} %convert_bitcast_fusion) | copy-start | bytes 6148
  20.7 9.1 %copy-start.31 = (f32[128,4]{0,1:T(4,128)S(1)}, f32[128,4]{0,1:T(4,128)}, u32[]{:S(2)}) copy-start(f32[128,4]{0,1:T(4,128)} %param.41) | copy-start | bytes 6148
  20.7 9.7 %copy-start.3 = (f32[2,128,2,8]{3,2,1,0:T(2,128)S(1)}, f32[2,128,2,8]{3,2,1,0:T(2,128)}, u32[]{:S(2)}) copy-start(f32[2,128,2,8]{3,2,1,0:T(2,128)} %copy-done.2) | copy-start | bytes 49156
  20.7 10.4 %copy-start.9 = (f32[2,128,2,8]{3,2,1,0:T(2,128)S(1)}, f32[2,128,2,8]{3,2,1,0:T(2,128)}, u32[]{:S(2)}) copy-start(f32[2,128,2,8]{3,2,1,0:T(2,128)} %get-tuple-element.30) | copy-start | bytes 49156
  25.6 5.5 %copy-start.24 = (f32[16]{0:T(128)}, f32[16]{0:T(128)S(1)}, u32[]{:S(2)}) copy-start(f32[16]{0:T(128)S(1)} %get-tuple-element.26) | copy-start | bytes 196
  28.5 8.3 %collective-permute-start.2 = (bf16[1040,128]{1,0:T(8,128)(2,1)}, bf16[1040,128]{1,0:T(8,128)(2,1)}, u32[]{:S(2)}, u32[]{:S(2)}) collective-permute-start(bf16[1040,128]{1,0:T(8,128)(2,1)} %pad_maximum_fusion.1), channel_id=1, source_target_pairs={{0,4},{2,6},{4,0},{6,2},{8,12},{10,14},{12,8},{14,10},{16,20},{18,... | collective-permute-start | bytes 798728 | tf_op jit(solution)/shard_map/ppermute | solution.py:24
  40.6 7.9 %copy-start = (f32[1024,128]{1,0:T(8,128)S(1)}, f32[1024,128]{1,0:T(8,128)}, u32[]{:S(2)}) copy-start(f32[1024,128]{1,0:T(8,128)} %get-tuple-element.25) | copy-start | bytes 1572868
  42.1 5.9 %collective-permute-start.3 = (bf16[1040,128]{1,0:T(8,128)(2,1)S(1)}, bf16[1040,128]{1,0:T(8,128)(2,1)S(1)}, u32[]{:S(2)}, u32[]{:S(2)}) collective-permute-start(bf16[1040,128]{1,0:T(8,128)(2,1)S(1)} %pad_maximum_fusion.2), channel_id=1, source_target_pairs={{0,8},{2,10},{4,12},{6,14},{8,0},{10,2},{12,4},{14,6},{16,24},{18,... | collective-permute-start | bytes 798728 | tf_op jit(solution)/shard_map/ppermute | solution.py:24
  42.3 7.0 %copy-start.19 = (pred[128]{0:T(512)(128)(4,1)S(1)}, pred[128]{0:T(512)(128)(4,1)}, u32[]{:S(2)}) copy-start(pred[128]{0:T(512)(128)(4,1)} %copy-done.17) | copy-start | bytes 388
  42.3 7.0 %copy-start.22 = (pred[128]{0:T(512)(128)(4,1)S(1)}, pred[128]{0:T(512)(128)(4,1)}, u32[]{:S(2)}) copy-start(pred[128]{0:T(512)(128)(4,1)} %copy-done.20) | copy-start | bytes 388
  42.5 8.4 %copy-start.13 = (f32[2,128,2,8]{1,3,0,2:T(8,128)S(1)}, f32[2,128,2,8]{1,3,0,2:T(8,128)}, u32[]{:S(2)}) copy-start(f32[2,128,2,8]{1,3,0,2:T(8,128)} %get-tuple-element.34) | copy-start | bytes 49156
  42.5 8.4 %copy-start.15 = (f32[2,2,8,128]{3,2,1,0:T(8,128)S(1)}, f32[2,2,8,128]{3,2,1,0:T(8,128)}, u32[]{:S(2)}) copy-start(f32[2,2,8,128]{3,2,1,0:T(8,128)} %copy.122) | copy-start | bytes 49156
  42.5 8.4 %copy-start.16 = (pred[128,128]{1,0:T(8,128)(4,1)S(1)}, pred[128,128]{1,0:T(8,128)(4,1)}, u32[]{:S(2)}) copy-start(pred[128,128]{1,0:T(8,128)(4,1)} %iota_compare_fusion) | copy-start | bytes 49156
  49.4 16.2 %collective-permute-start.4 = (bf16[1040,128]{1,0:T(8,128)(2,1)S(1)}, bf16[1040,128]{1,0:T(8,128)(2,1)}, u32[]{:S(2)}, u32[]{:S(2)}) collective-permute-start(bf16[1040,128]{1,0:T(8,128)(2,1)S(1)} %pad_maximum_fusion.3), channel_id=1, source_target_pairs={{0,16},{2,18},{4,20},{6,22},{8,24},{10,26},{12,28},{14,30},{1,17},... | collective-permute-start | bytes 798728 | tf_op jit(solution)/shard_map/ppermute | solution.py:24
  52.9 13.8 %copy-start.7 = (f32[1024,128]{1,0:T(8,128)S(1)}, f32[1024,128]{1,0:T(8,128)}, u32[]{:S(2)}) copy-start(f32[1024,128]{1,0:T(8,128)} %get-tuple-element.29) | copy-start | bytes 1572868
  54.2 12.8 %copy-start.4 = (f32[2,2,8,64,128]{4,3,2,1,0:T(8,128)S(1)}, f32[2,2,8,64,128]{4,3,2,1,0:T(8,128)}, u32[]{:S(2)}) copy-start(f32[2,2,8,64,128]{4,3,2,1,0:T(8,128)} %get-tuple-element.53) | copy-start | bytes 3145732
  54.2 12.8 %copy-start.28 = (f32[2,8]{1,0:T(2,128)S(1)}, f32[2,8]{1,0:T(2,128)}, u32[]{:S(2)}) copy-start(f32[2,8]{1,0:T(2,128)} %fusion.40) | copy-start | bytes 196
  (5 other events, 6.4 us)

commit v2 on v1

--- a/solution.py
+++ b/solution.py
@@ -7,65 +7,8 @@
 from jax.experimental.pallas import tpu as pltpu
 from jax.sharding import PartitionSpec as P
 
-HEAD_DIM = 64
 STATE = 128
 BLK = 128
-
-
-def from_behind(block, axis, distance):
-    devices = range(lax.axis_size(axis))
-    route = [(i - distance, i) for i in devices if i - distance in devices]
-    return lax.ppermute(block, axis, route)
-
-
-def swap(block, axis, step, upward_only):
-    devices = range(lax.axis_size(axis))
-    route = [(i, i ^ step) for i in devices if not (upward_only and i & step)]
-    return lax.ppermute(block, axis, route)
-
-
-def carried_in(log_total, state, axis):
-    count, mine = lax.axis_size(axis), lax.axis_index(axis)
-    heads, width = log_total.size, state.shape[-1]
-    flat = state.reshape(heads, -1, width)
-    decay = jnp.exp(log_total).reshape(heads)
-    total, before, before_decay = flat, jnp.zeros_like(flat), jnp.ones_like(decay)
-    step = 1
-    while step < count:
-        coarse = lax.reduce_precision(decay, 8, 7)
-        lane = jnp.arange(width)[None, :]
-        tail = jnp.where(lane == 0, coarse[:, None], jnp.where(lane == 1, (decay - coarse)[:, None], 0.0))
-        sent = jnp.concatenate([total.reshape(-1, width), tail], axis=0).astype(jnp.bfloat16)
-        got = swap(sent, axis, step, 2 * step >= count).astype(jnp.float32)
-        other = got[: got.shape[0] - heads].reshape(flat.shape)
-        other_decay = got[got.shape[0] - heads :, 0] + got[got.shape[0] - heads :, 1]
-        upper = (mine & step) != 0
-        before = before + jnp.where(upper, before_decay, 0.0)[:, None, None] * other
-        if 2 * step < count:
-            before_decay = before_decay * jnp.where(upper, other_decay, 1.0)
-            total = jnp.where(
-                upper, other * decay[:, None, None] + total, total * other_decay[:, None, None] + other
-            )
-            decay = decay * other_decay
-        step *= 2
-    return before.reshape(state.shape)
-
-
-def causal_conv(previous, current, weight):
-    stacked = jnp.concatenate([previous, current], axis=0).astype(jnp.float32)
-    weight = weight.astype(jnp.float32)
-    kernel_len = weight.shape[0]
-    length = current.shape[0]
-    summed_taps = weight[0] * stacked[0:length]
-    for offset in range(1, kernel_len):
-        summed_taps = summed_taps + weight[offset] * stacked[offset : offset + length]
-    return jax.nn.silu(summed_taps)
-
-
-def product(spec, *operands):
-    return jnp.einsum(
-        spec, *[part.astype(jnp.bfloat16) for part in operands], preferred_element_type=jnp.float32
-    )
 
 
 MESH = pl.DeviceIdType.MESH
@@ -612,6 +555,414 @@
     )
 
 
+def mixer_stage(
+    heads,
+    groups,
+    owners,
+    head_dim,
+    signal_in,
+    write_in,
+    read_in,
+    gate_in,
+    step_in,
+    log_in,
+    signal_taps,
+    write_taps,
+    read_taps,
+    bias,
+    rate,
+    direct,
+    gain,
+    mixed,
+    halo_signal,
+    halo_write,
+    halo_read,
+    extended,
+    signal,
+    write_vec,
+    read_vec,
+    scaled,
+    tailed,
+    readout,
+    states,
+    summed,
+    piece_out,
+    piece_in,
+    decay_out,
+    decay_in,
+    start_out,
+    start_in,
+    halo_send,
+    halo_recv,
+    piece_send,
+    piece_recv,
+    decay_send,
+    decay_recv,
+    start_send,
+    start_recv,
+):
+    chip, core = lax.axis_index("sp"), lax.axis_index("tp")
+    chips = lax.axis_size("sp")
+    length, wide = signal_in.shape
+    narrow = write_in.shape[1]
+    rim = halo_signal.shape[0]
+    taps = signal_taps.shape[0]
+    blocks = length // BLK
+    per_group = heads // groups
+    span = per_group * head_dim
+    rows = STATE // owners
+    f32, bf16 = jnp.float32, jnp.bfloat16
+    exact = lax.Precision.HIGHEST
+
+    def halo_copies(target):
+        return [
+            pltpu.make_async_remote_copy(
+                src_ref=source.at[pl.ds(length - rim, rim), :],
+                dst_ref=halo,
+                send_sem=halo_send.at[number],
+                recv_sem=halo_recv.at[number],
+                device_id=(target, core),
+                device_id_type=MESH,
+            )
+            for number, (source, halo) in enumerate(
+                [(signal_in, halo_signal), (write_in, halo_write), (read_in, halo_read)]
+            )
+        ]
+
+    @pl.when(chip < chips - 1)
+    def _():
+        for copy in halo_copies(chip + 1):
+            copy.start()
+
+    timestep = step_in[...].astype(f32) + bias[...]
+    timestep = jnp.maximum(timestep, 0.0) + jnp.log1p(jnp.exp(-jnp.abs(timestep)))
+    log_decay = log_in[...] - rate[...] * timestep
+    first = lax.broadcasted_iota(jnp.int32, (BLK, BLK), 0)
+    second = lax.broadcasted_iota(jnp.int32, (BLK, BLK), 1)
+    causal = first >= second
+    lower = jnp.where(causal, 1.0, 0.0)
+    cums = [
+        jnp.dot(
+            lower,
+            log_decay[b * BLK : (b + 1) * BLK],
+            precision=exact,
+            preferred_element_type=f32,
+        )
+        for b in range(blocks)
+    ]
+    part = lax.broadcasted_iota(jnp.int32, (heads, wide), 0)
+    lane = lax.broadcasted_iota(jnp.int32, (heads, wide), 1) // head_dim
+    widen = jnp.where(part == lane, 1.0, 0.0).astype(bf16)
+
+    def expand(value):
+        high = value.astype(bf16)
+        rest = value - high.astype(f32)
+        middle = rest.astype(bf16)
+        low = (rest - middle.astype(f32)).astype(bf16)
+        return (
+            jnp.dot(high, widen, preferred_element_type=f32)
+            + jnp.dot(middle, widen, preferred_element_type=f32)
+            + jnp.dot(low, widen, preferred_element_type=f32)
+        )
+
+    for b in range(blocks):
+        readout[b * BLK : (b + 1) * BLK, :] = expand(jnp.exp(cums[b]))
+    decay = readout[BLK - 1 : BLK, :]
+    for b in range(1, blocks):
+        decay = decay * readout[(b + 1) * BLK - 1 : (b + 1) * BLK, :]
+    decay_out[...] = decay
+
+    def decay_copy(owner, device):
+        return pltpu.make_async_remote_copy(
+            src_ref=decay_out,
+            dst_ref=decay_in.at[device],
+            send_sem=decay_send.at[owner],
+            recv_sem=decay_recv.at[device],
+            device_id=(owner, core),
+            device_id_type=MESH,
+        )
+
+    def piece_copy(owner, device):
+        return pltpu.make_async_remote_copy(
+            src_ref=piece_out.at[owner],
+            dst_ref=piece_in.at[device],
+            send_sem=piece_send.at[owner],
+            recv_sem=piece_recv.at[device],
+            device_id=(owner, core),
+            device_id_type=MESH,
+        )
+
+    def start_copy(owner, device):
+        return pltpu.make_async_remote_copy(
+            src_ref=start_out.at[device],
+            dst_ref=start_in.at[owner],
+            send_sem=start_send.at[device],
+            recv_sem=start_recv.at[owner],
+            device_id=(device, core),
+            device_id_type=MESH,
+        )
+
+    def others(number, act):
+        for at in range(number):
+
+            @pl.when(at != chip)
+            def _():
+                act(at)
+
+    others(owners, lambda owner: decay_copy(owner, chip).start())
+
+    @pl.when(chip < owners)
+    def _():
+        decay_in[chip] = decay_out[...]
+
+    parts = [
+        (signal_in, halo_signal, signal_taps, 0, wide),
+        (write_in, halo_write, write_taps, wide, narrow),
+        (read_in, halo_read, read_taps, wide + narrow, narrow),
+    ]
+    head_room = 8
+    for source, _, _, at, size in parts:
+        extended[head_room : head_room + length, at : at + size] = source[...].astype(f32)
+
+    @pl.when(chip > 0)
+    def _():
+        for copy in halo_copies(chip):
+            copy.wait_recv()
+        for _, halo, _, at, size in parts:
+            extended[0:head_room, at : at + size] = halo[rim - head_room : rim, :].astype(f32)
+
+    @pl.when(chip == 0)
+    def _():
+        extended[0:head_room, :] = jnp.zeros((head_room, extended.shape[1]), f32)
+
+    def convolve(weights, at, size, put):
+        for b in range(blocks):
+            for lanes in range(0, size, 256):
+                total = None
+                for tap in range(taps):
+                    begin = head_room - taps + 1 + tap + b * BLK
+                    term = (
+                        weights[tap : tap + 1, lanes : lanes + 256].astype(f32)
+                        * extended[begin : begin + BLK, at + lanes : at + lanes + 256]
+                    )
+                    total = term if total is None else total + term
+                put(b, lanes, jax.nn.silu(total))
+
+    def put_write(b, lanes, value):
+        write_vec[b * BLK : (b + 1) * BLK, lanes : lanes + 256] = value.astype(bf16)
+
+    def put_read(b, lanes, value):
+        read_vec[b * BLK : (b + 1) * BLK, lanes : lanes + 256] = value.astype(bf16)
+
+    def put_signal(b, lanes, value):
+        signal[b * BLK : (b + 1) * BLK, lanes : lanes + 256] = value
+
+    convolve(write_taps, wide, narrow, put_write)
+    convolve(signal_taps, 0, wide, put_signal)
+    for b in range(blocks):
+        spot = slice(b * BLK, (b + 1) * BLK)
+        step = timestep[spot]
+        scaled[spot, :] = (signal[spot, :] * expand(step)).astype(bf16)
+        rest = jnp.exp(cums[b][BLK - 1 : BLK, :] - cums[b])
+        tailed[spot, :] = (signal[spot, :] * expand(step * rest)).astype(bf16)
+        for g in range(groups):
+            states[b, :, g * span : (g + 1) * span] = lax.dot_general(
+                write_vec[spot, g * STATE : (g + 1) * STATE],
+                tailed[spot, g * span : (g + 1) * span],
+                (((0,), (0,)), ((), ())),
+                preferred_element_type=f32,
+            )
+    for owner in range(owners):
+        spot = slice(owner * rows, (owner + 1) * rows)
+        value = states[0, spot, :]
+        for b in range(1, blocks):
+            value = value * readout[(b + 1) * BLK - 1 : (b + 1) * BLK, :] + states[b, spot, :]
+        piece_out[owner] = value.astype(bf16)
+    others(owners, lambda owner: piece_copy(owner, chip).start())
+
+    @pl.when(chip < owners)
+    def _():
+        piece_in[chip] = piece_out[chip]
+
+    convolve(read_taps, wide + narrow, narrow, put_read)
+    spread_direct = expand(jnp.broadcast_to(direct[...], (8, heads)))[0:1, :]
+    low_lanes = lax.broadcasted_iota(jnp.int32, (BLK, 2 * head_dim), 1) < head_dim
+    for b in range(blocks):
+        spot = slice(b * BLK, (b + 1) * BLK)
+        turned = cums[b].T
+        for g in range(groups):
+            inner = slice(g * STATE, (g + 1) * STATE)
+            meeting = lax.dot_general(
+                read_vec[spot, inner],
+                write_vec[spot, inner],
+                (((1,), (1,)), ((), ())),
+                preferred_element_type=f32,
+            )
+            for pair in range(per_group // 2):
+                head = g * per_group + 2 * pair
+                lanes = slice(head * head_dim, (head + 2) * head_dim)
+                weights = []
+                for at in (head, head + 1):
+                    gap = cums[b][:, at : at + 1] - turned[at : at + 1, :]
+                    weights.append(
+                        (meeting * jnp.exp(jnp.where(causal, gap, -jnp.inf))).astype(bf16)
+                    )
+                value = scaled[spot, lanes]
+                zero = jnp.zeros_like(value)
+                both = jnp.concatenate(
+                    [jnp.where(low_lanes, value, zero), jnp.where(low_lanes, zero, value)], axis=0
+                )
+                summed[spot, lanes] = spread_direct[:, lanes] * signal[spot, lanes] + jnp.dot(
+                    jnp.concatenate(weights, axis=1), both, preferred_element_type=f32
+                )
+
+    @pl.when(chip < owners)
+    def _():
+        def scan(device, held):
+            @pl.when(device != chip)
+            def _():
+                decay_copy(chip, device).wait_recv()
+                piece_copy(chip, device).wait_recv()
+
+            start_out[device] = held.astype(bf16)
+
+            @pl.when(device != chip)
+            def _():
+                start_copy(chip, device).start()
+
+            return held * decay_in[device] + piece_in[device].astype(f32)
+
+        lax.fori_loop(0, chips, scan, jnp.zeros((rows, wide), f32))
+        start_in[chip] = start_out[chip]
+
+    others(owners, lambda owner: start_copy(owner, chip).wait_recv())
+    start = jnp.concatenate([start_in[owner].astype(f32) for owner in range(owners)], axis=0)
+    for b in range(blocks):
+        spot = slice(b * BLK, (b + 1) * BLK)
+        if b:
+            start = (
+                start * readout[b * BLK - 1 : b * BLK, :] + states[b - 1]
+            )
+        rounded = start.astype(bf16)
+        for g in range(groups):
+            lanes = slice(g * span, (g + 1) * span)
+            near = jnp.dot(
+                read_vec[spot, g * STATE : (g + 1) * STATE],
+                rounded[:, lanes],
+                preferred_element_type=f32,
+            )
+            value = summed[spot, lanes] + near * readout[spot, lanes]
+            value = value * jax.nn.silu(gate_in[spot, lanes].astype(f32))
+            scale = lax.rsqrt(jnp.mean(value * value, axis=-1, keepdims=True) + 1e-06)
+            mixed[spot, lanes] = (value * scale * gain[:, lanes]).astype(bf16)
+
+    @pl.when(chip < chips - 1)
+    def _():
+        for copy in halo_copies(chip + 1):
+            copy.wait_send()
+
+    others(owners, lambda owner: decay_copy(owner, chip).wait_send())
+    others(owners, lambda owner: piece_copy(owner, chip).wait_send())
+
+    @pl.when(chip < owners)
+    def _():
+        others(chips, lambda device: start_copy(chip, device).wait_send())
+
+
+def mixer_scratch(chips, owners, length, wide, narrow, blocks):
+    f32, bf16 = jnp.float32, jnp.bfloat16
+    dma = pltpu.SemaphoreType.DMA
+    rows = STATE // owners
+    rim = 16
+    return [
+        pltpu.VMEM((rim, wide), bf16),
+        pltpu.VMEM((rim, narrow), bf16),
+        pltpu.VMEM((rim, narrow), bf16),
+        pltpu.VMEM((length + 8, wide + 2 * narrow), f32),
+        pltpu.VMEM((length, wide), f32),
+        pltpu.VMEM((length, narrow), bf16),
+        pltpu.VMEM((length, narrow), bf16),
+        pltpu.VMEM((length, wide), bf16),
+        pltpu.VMEM((length, wide), bf16),
+        pltpu.VMEM((length, wide), f32),
+        pltpu.VMEM((blocks, STATE, wide), f32),
+        pltpu.VMEM((length, wide), f32),
+        pltpu.VMEM((owners, rows, wide), bf16),
+        pltpu.VMEM((chips, rows, wide), bf16),
+        pltpu.VMEM((1, wide), f32),
+        pltpu.VMEM((chips, 1, wide), f32),
+        pltpu.VMEM((chips, rows, wide), bf16),
+        pltpu.VMEM((owners, rows, wide), bf16),
+        dma((3,)),
+        dma((3,)),
+        dma((owners,)),
+        dma((chips,)),
+        dma((owners,)),
+        dma((chips,)),
+        dma((chips,)),
+        dma((owners,)),
+    ]
+
+
+def mixer_kernel(heads, groups, owners, head_dim, *refs):
+    chip, core = lax.axis_index("sp"), lax.axis_index("tp")
+    chips = lax.axis_size("sp")
+    barrier = pltpu.get_barrier_semaphore()
+    for ahead in range(1, chips):
+        pl.semaphore_signal(
+            barrier, inc=1, device_id=((chip + ahead) % chips, core), device_id_type=MESH
+        )
+    pl.semaphore_wait(barrier, chips - 1)
+    mixer_stage(heads, groups, owners, head_dim, *refs)
+
+
+def mixer(
+    signal_in,
+    write_in,
+    read_in,
+    gate_in,
+    step_in,
+    log_in,
+    signal_taps,
+    write_taps,
+    read_taps,
+    bias,
+    rate,
+    direct,
+    gain,
+):
+    chips = lax.axis_size("sp")
+    length, wide = signal_in.shape
+    narrow = write_in.shape[1]
+    heads = step_in.shape[1]
+    owners = min(chips, STATE // 8)
+    vmem = pl.BlockSpec(memory_space=pltpu.VMEM)
+    return pl.pallas_call(
+        functools.partial(mixer_kernel, heads, narrow // STATE, owners, wide // heads),
+        out_shape=jax.ShapeDtypeStruct((length, wide), jnp.bfloat16),
+        in_specs=[vmem] * 13,
+        out_specs=vmem,
+        scratch_shapes=mixer_scratch(chips, owners, length, wide, narrow, length // BLK),
+        compiler_params=pltpu.CompilerParams(
+            collective_id=1, has_side_effects=True, vmem_limit_bytes=60 * 2**20
+        ),
+    )(
+        signal_in,
+        write_in,
+        read_in,
+        gate_in,
+        step_in,
+        log_in,
+        signal_taps,
+        write_taps,
+        read_taps,
+        bias.reshape(1, -1),
+        rate.reshape(1, -1),
+        direct.reshape(1, -1),
+        gain.reshape(1, -1),
+    )
+
+
 def on_device(
     stream,
     head_input_signal,
@@ -638,64 +989,21 @@
     common_up_weight,
     common_down_weight,
 ):
-    length = head_input_signal.shape[0]
-    margin = signal_filter_taps.shape[0] - 1
-    head_count = step_size_input.shape[1]
-    groups = write_input_vectors.shape[1] // STATE
-    per_group = head_count // groups
-    blocks = length // BLK
-    wide, narrow = head_input_signal.shape[1], write_input_vectors.shape[1]
-    rim = jnp.concatenate(
-        [part[length - margin :] for part in (head_input_signal, write_input_vectors, read_input_vectors)],
-        axis=1,
+    mixer_out = mixer(
+        head_input_signal,
+        write_input_vectors,
+        read_input_vectors,
+        output_gate_input,
+        step_size_input,
+        position_log_decay,
+        signal_filter_taps,
+        write_filter_taps,
+        read_filter_taps,
+        step_size_bias,
+        head_decay_rate,
+        head_direct_term,
+        grouped_norm_gain,
     )
-    rim = from_behind(rim, "sp", 1)
-    before = (rim[:, :wide], rim[:, wide : wide + narrow], rim[:, wide + narrow :])
-    signal = causal_conv(before[0], head_input_signal, signal_filter_taps)
-    write_vec = causal_conv(before[1], write_input_vectors, write_filter_taps)
-    read_vec = causal_conv(before[2], read_input_vectors, read_filter_taps)
-    time_position = jax.nn.softplus(step_size_input.astype(jnp.float32) + step_size_bias)
-    decay_logarithm = position_log_decay - head_decay_rate * time_position
-    signal_heads = signal.reshape(blocks, BLK, groups, per_group, HEAD_DIM)
-    scaled_blocks = signal_heads * time_position.reshape(blocks, BLK, groups, per_group)[..., None]
-    write_blocks = write_vec.reshape(blocks, BLK, groups, STATE)
-    read_blocks = read_vec.reshape(blocks, BLK, groups, STATE)
-    within_cum = jnp.cumsum(decay_logarithm.reshape(blocks, BLK, groups, per_group), axis=1)
-    block_total = within_cum[:, -1]
-    running = jnp.cumsum(block_total, axis=0)
-    device_total = running[-1]
-    causal = jnp.arange(BLK)[:, None] >= jnp.arange(BLK)[None, :]
-    cum_heads = jnp.transpose(within_cum, (0, 2, 3, 1))
-    differences = cum_heads[..., :, None] - cum_heads[..., None, :]
-    decay_matrix = jnp.exp(jnp.where(causal, differences, -jnp.inf))
-    tail_decay = jnp.exp(block_total[:, None] - within_cum)
-    block_states = product(
-        "bsgn,bsgep->bgepn", write_blocks, scaled_blocks * tail_decay[..., None]
-    )
-    device_state = jnp.sum(
-        block_states * jnp.exp(device_total[None] - running)[..., None, None], axis=0
-    )
-    incoming = carried_in(device_total, device_state, "sp")
-    intersection = product("btgn,bsgn->bgts", read_blocks, write_blocks)
-    intra_out = product(
-        "bgets,bsgep->btgep", intersection[:, :, None] * decay_matrix, scaled_blocks
-    )
-    readout_scale = jnp.exp(within_cum)
-    starts = [incoming]
-    for block in range(blocks - 1):
-        starts.append(
-            starts[-1] * jnp.exp(block_total[block])[..., None, None] + block_states[block]
-        )
-    near_out = (
-        product("btgn,bgepn->btgep", read_blocks, jnp.stack(starts)) * readout_scale[..., None]
-    )
-    ssd_out = intra_out + near_out
-    ssd_out = ssd_out + head_direct_term.reshape(groups, per_group)[:, :, None] * signal_heads
-    gated = ssd_out.reshape(length, groups, per_group * HEAD_DIM) * jax.nn.silu(
-        output_gate_input.astype(jnp.float32)
-    ).reshape(length, groups, per_group * HEAD_DIM)
-    norm_scale = lax.rsqrt(jnp.mean(gated * gated, axis=-1, keepdims=True) + 1e-06)
-    mixer_out = ((gated * norm_scale).reshape(length, -1) * grouped_norm_gain).astype(jnp.bfloat16)
     return tail(
         mixer_out,
         stream,

time: 200 us -> 157 us (0.79)
  the two profiles are of different devices: /device:TPU:25 before, /device:TPU:27 now
where the time goes in v2:
time: 157 us
  Pallas kernels  150 us (96%)
  local copies, waits for them, and re-layouts  4.77 us (3%)
  other arithmetic  1.96 us (1%)
    pallas_call x1, Pallas kernels, tail(): pl.pallas_call(functools.partial(tail_kernel, planes, ring, tp_count, cap...  126 us
    pallas_call x1, Pallas kernels, mixer(): pl.pallas_call(functools.partial(mixer_kernel, heads, narrow // STATE, ow...  23.5 us
    unnamed x3, local copies, waits for them, and re-layouts  4.77 us

profile of v2, /device:TPU:27, one launch (start us, length us, event | category | flops | bytes accessed | tf_op | source)
XLA Modules:
  0.0 156.6 jit_solution(17220740016632040627)
XLA Ops:
  0.0 0.7 convert_bitcast_fusion
  0.7 1.3 pad_maximum_fusion.table_ref
  2.0 1.4 copy.25.refs_4_
  3.4 1.5 copy.26.refs_5_
  4.9 23.5 %shard_map.226.mixed_ref = bf16[256,1024]{1,0:T(8,128)(2,1)} custom-call(bf16[256,1024]{1,0:T(8,128)(2,1)} %refs_0_.1, bf16[256,256]{1,0:T(8,128)(2,1)} %refs_1_.1, bf16[256,256]{1,0:T(8,128)(2,1)} %refs_2_.1, bf16[256,1024]{1,0:T(8,128)(2,1)} %refs_3_.1, bf16[256,16]{1,0:T(8,128)(2,1)} %copy.25.refs_4_, f32[256,16]{1,0:T(8,128)} %copy.26.refs_5_, ...), custom_call_target="tpu_custom_call" | custom-call | tf_op jit(solution)/shard_map/pallas_call | solution.py:940
  28.4 126.3 %shard_map.227 = bf16[128,2048]{1,0:T(8,128)(2,1)} custom-call(bf16[256,1024]{1,0:T(8,128)(2,1)} %shard_map.226.mixed_ref, bf16[128,2048]{1,0:T(8,128)(2,1)} %stream_ref.1, f32[1,2048]{1,0:T(1,128)} %bitcast.8, f32[8,128]{1,0:T(8,128)} %pad_maximum_fusion.table_ref, bf16[1024,2048]{1,0:T(8,128)(2,1)} %out_weight_hbm.1, bf16[1,2048,512]{2,1,0:T(8,128)(2,1)} %gate_hbm.1, ...), custom_call_target="tpu_custom_call" | custom-call | tf_op jit(solution)/shard_map/pallas_call | solution.py:498
  154.7 1.9 %copy.28 = bf16[128,2048]{1,0:T(8,128)(2,1)} copy(bf16[128,2048]{1,0:T(8,128)(2,1)} %shard_map.227) | data formatting | bytes 1048576

commit v3 on v2

--- a/solution.py
+++ b/solution.py
@@ -16,12 +16,28 @@
 COLS = 512
 
 
+LINE_END = [(0, 0), (0, 1), (3, 0), (0, 2), (1, 1), (1, 2), (0, 3), (2, 2), (2, 1), (1, 3), (2, 3), (1, 0), (2, 0)]
+LINE_NEXT = [(0, 1), (0, 2), (0, 0), (3, 0), (1, 2), (0, 3), (2, 2), (1, 0), (1, 3), (2, 0), (2, 3), (1, 1), (2, 1)]
+
+
+def line_plans(planes):
+    if planes == 4:
+        mirror = lambda plan: [(kind, 3 - owner) for kind, owner in plan]
+        plans = [LINE_END, LINE_NEXT, mirror(LINE_NEXT), mirror(LINE_END)]
+    else:
+        plans = []
+        for z in range(planes):
+            near = sorted(range(planes), key=lambda s: (abs(s - z), s))
+            plans.append([(0, s) for s in near] + [(3, 0)] + [(k, s) for s in near for k in (1, 2)])
+    return [[kind * planes + owner for kind, owner in plan] for plan in plans]
+
+
 def column_chunks(width):
     step = min(COLS, width)
     return [(at, step) for at in range(0, width, step)]
 
 
-def pick(values, place, which, index):
+def pick(values, place, which):
     chosen = jnp.int32(0)
     for spot, row in enumerate(values):
         chosen = chosen + (place == spot).astype(jnp.int32) * pick_one(row, which)
@@ -44,7 +60,8 @@
     mixed_ref,
     stream_ref,
     gain_ref,
-    table_ref,
+    index_ref,
+    weight_ref,
     out_weight_hbm,
     gate_hbm,
     up_hbm,
@@ -60,7 +77,8 @@
     common_gate,
     common_up,
     common_down,
-    tables,
+    index_tables,
+    weight_tables,
     total,
     residual,
     part_out,
@@ -95,7 +113,7 @@
     plane = chip // chips
     mine = (chip % chips) * tp_count + core
     count, width = rows.shape[1], rows.shape[2]
-    order = [sorted(range(planes), key=lambda s: (abs(s - z), s)) for z in range(planes)]
+    plans = line_plans(planes)
 
     def in_plane(spot):
         return (plane * chips + spot // tp_count, spot % tp_count)
@@ -131,19 +149,26 @@
         )
     pl.semaphore_wait(barrier, ring + planes - 2)
 
-    def table_copy(ahead, owner):
-        return pltpu.make_async_remote_copy(
-            src_ref=table_ref,
-            dst_ref=tables.at[owner],
-            send_sem=table_send.at[ahead],
-            recv_sem=table_recv.at[owner],
-            device_id=in_line((plane + ahead) % planes),
-            device_id_type=MESH,
-        )
+    def table_copies(ahead, owner):
+        return [
+            pltpu.make_async_remote_copy(
+                src_ref=source,
+                dst_ref=held.at[owner],
+                send_sem=table_send.at[number, ahead],
+                recv_sem=table_recv.at[number, owner],
+                device_id=in_line((plane + ahead) % planes),
+                device_id_type=MESH,
+            )
+            for number, (source, held) in enumerate(
+                [(index_ref, index_tables), (weight_ref, weight_tables)]
+            )
+        ]
 
     for ahead in range(1, planes):
-        table_copy(ahead, plane).start()
-    tables[plane] = table_ref[...]
+        for copy in table_copies(ahead, plane):
+            copy.start()
+    index_tables[plane] = index_ref[...]
+    weight_tables[plane] = weight_ref[...]
 
     def part_copy(ahead):
         return pltpu.make_async_remote_copy(
@@ -262,15 +287,14 @@
         )
 
     def slots_of(owner):
-        table = tables[owner]
-        first = (plane * ring).astype(jnp.float32)
-        names = lax.broadcasted_iota(jnp.int32, (ring, count), 0).astype(jnp.float32) + first
+        table, parts = index_tables[owner], weight_tables[owner]
+        names = lax.broadcasted_iota(jnp.int32, (ring, count), 0) + plane * ring
         hits = jnp.zeros((ring, count), jnp.float32)
         share = jnp.zeros((ring, count), jnp.float32)
         for turn in range(fanout):
             named = table[turn : turn + 1, :] == names
             hits = hits + jnp.where(named, 1.0, 0.0)
-            share = share + jnp.where(named, table[fanout + turn : fanout + turn + 1, :], 0.0)
+            share = share + jnp.where(named, parts[turn : turn + 1, :], 0.0)
         before = lax.broadcasted_iota(jnp.int32, (count, count), 0)
         after = lax.broadcasted_iota(jnp.int32, (count, count), 1)
         earlier = jnp.where(before < after, 1.0, 0.0).astype(jnp.bfloat16)
@@ -281,7 +305,8 @@
 
     def wait_table(owner):
         ahead = (owner + planes - plane) % planes
-        table_copy(ahead, owner).wait_recv()
+        for copy in table_copies(ahead, owner):
+            copy.wait_recv()
 
     def dispatch(owner):
         @pl.when(owner != plane)
@@ -401,35 +426,40 @@
         def _():
             sums_copy(owner).start()
 
-    def source(turn):
-        return pick(order, plane, turn, 0)
+    def share_expert():
+        for load in loads[1:4]:
+            load.wait()
+
+        def put(at, step, value):
+            total[:, at : at + step] += value
+
+        ffn(rows.at[plane], common_gate, common_up, common_down, residual, put)
 
     def step(turn, carry):
-        @pl.when(turn < planes)
+        code = pick(plans, plane, turn)
+        kind, owner = code // planes, code % planes
+
+        @pl.when(kind == 0)
         def _():
-            dispatch(source(turn))
-
-        @pl.when(turn == 0)
+            dispatch(owner)
+
+        @pl.when(kind == 1)
         def _():
-            for load in loads[1:]:
-                load.wait()
-
-            def put(at, step, value):
-                total[:, at : at + step] += value
-
-            ffn(rows.at[plane], common_gate, common_up, common_down, residual, put)
-
-        @pl.when((turn >= 1) & (turn <= planes))
+            serve(owner)
+
+        @pl.when(kind == 2)
         def _():
-            serve(source(turn - 1))
-
-        @pl.when(turn >= 2)
+            collect(owner)
+
+        @pl.when(kind == 3)
         def _():
-            collect(source(turn - 2))
+            share_expert()
 
         return carry
 
-    lax.fori_loop(0, planes + 2, step, 0)
+    for load in loads[4:]:
+        load.wait()
+    lax.fori_loop(0, len(plans[0]), step, 0)
 
     for ahead in range(1, planes):
         sums_wait((plane + ahead) % planes).wait_recv()
@@ -447,7 +477,8 @@
     for ahead in range(1, tp_count):
         part_copy(ahead).wait_send()
     for ahead in range(1, planes):
-        table_copy(ahead, plane).wait_send()
+        for copy in table_copies(ahead, plane):
+            copy.wait_send()
         sums_copy((plane + ahead) % planes).wait_send()
     for owner in range(planes):
 
@@ -490,7 +521,6 @@
     experts = sp_count * tp_count
     capacity = max(2, (3 * count * fanout + 2 * experts - 1) // (2 * experts))
     capacity = (capacity + 7) // 8 * 8
-    table = jnp.concatenate([index.astype(jnp.float32).T, weight.T], axis=0)
     bf16 = jnp.bfloat16
     vmem, anywhere = pl.BlockSpec(memory_space=pltpu.VMEM), pl.BlockSpec(memory_space=pl.ANY)
     slots = (planes, ring, capacity, width)
@@ -498,7 +528,7 @@
     return pl.pallas_call(
         functools.partial(tail_kernel, planes, ring, tp_count, capacity, fanout),
         out_shape=jax.ShapeDtypeStruct((count, width), bf16),
-        in_specs=[vmem] * 4 + [anywhere] * 7,
+        in_specs=[vmem] * 5 + [anywhere] * 7,
         out_specs=vmem,
         scratch_shapes=[
             pltpu.VMEM(out_weight.shape, bf16),
@@ -508,7 +538,8 @@
             pltpu.VMEM(common_gate.shape, bf16),
             pltpu.VMEM(common_up.shape, bf16),
             pltpu.VMEM(common_down.shape, bf16),
-            pltpu.VMEM((planes, 2 * fanout, count), jnp.float32),
+            pltpu.VMEM((planes, fanout, count), jnp.int32),
+            pltpu.VMEM((planes, fanout, count), jnp.float32),
             pltpu.VMEM((count, width), jnp.float32),
             pltpu.VMEM((count, common_gate.shape[1]), bf16),
             pltpu.VMEM((tp_count - 1, count, width), bf16),
@@ -525,8 +556,8 @@
             dma((7,)),
             dma((tp_count - 1,)),
             dma((tp_count - 1,)),
-            dma((planes,)),
-            dma((planes,)),
+            dma((2, planes)),
+            dma((2, planes)),
             dma((planes,)),
             dma((planes,)),
             dma((planes,)),
@@ -544,7 +575,8 @@
         mixed,
         stream,
         gain.reshape(1, -1),
-        table,
+        index.T,
+        weight.T,
         out_weight,
         gate,
         up,
@@ -634,9 +666,9 @@
         for copy in halo_copies(chip + 1):
             copy.start()
 
-    timestep = step_in[...].astype(f32) + bias[...]
+    timestep = step_in[...].astype(f32).T + bias[...]
     timestep = jnp.maximum(timestep, 0.0) + jnp.log1p(jnp.exp(-jnp.abs(timestep)))
-    log_decay = log_in[...] - rate[...] * timestep
+    log_decay = log_in[...].T - rate[...] * timestep
     first = lax.broadcasted_iota(jnp.int32, (BLK, BLK), 0)
     second = lax.broadcasted_iota(jnp.int32, (BLK, BLK), 1)
     causal = first >= second
@@ -951,8 +983,8 @@
         write_in,
         read_in,
         gate_in,
-        step_in,
-        log_in,
+        step_in.T,
+        log_in.T,
         signal_taps,
         write_taps,
         read_taps,

time: 157 us -> 136 us (0.87)
  the two profiles are of different devices: /device:TPU:27 before, /device:TPU:0 now
where the time goes in v3:
time: 136 us; the launch traced here: 135 us
  Pallas kernels  133 us (98%)
  local copies, waits for them, and re-layouts  1.88 us (1%)
    pallas_call x1, Pallas kernels, tail(): pl.pallas_call(functools.partial(tail_kernel, planes, ring, tp_count, cap...  107 us
    pallas_call x1, Pallas kernels, mixer(): pl.pallas_call(functools.partial(mixer_kernel, heads, narrow // STATE, ow...  25.7 us

profile of v3, /device:TPU:0, one launch (start us, length us, event | category | flops | bytes accessed | tf_op | source)
XLA Modules:
  0.0 134.8 jit_solution(17832230963849134875)
XLA Ops:
  0.0 25.7 %shard_map.226.mixed_ref = bf16[256,1024]{1,0:T(8,128)(2,1)} custom-call(bf16[256,1024]{1,0:T(8,128)(2,1)} %refs_0_.1, bf16[256,256]{1,0:T(8,128)(2,1)} %refs_1_.1, bf16[256,256]{1,0:T(8,128)(2,1)} %refs_2_.1, bf16[256,1024]{1,0:T(8,128)(2,1)} %refs_3_.1, bf16[16,256]{1,0:T(8,128)(2,1)} %bitcast.10, f32[16,256]{1,0:T(8,128)} %bitcast.9, ...), custom_call_target="tpu_custom_call" | custom-call | tf_op jit(solution)/shard_map/pallas_call | solution.py:972
  25.7 107.2 %shard_map.227 = bf16[128,2048]{1,0:T(8,128)(2,1)} custom-call(bf16[256,1024]{1,0:T(8,128)(2,1)} %shard_map.226.mixed_ref, bf16[128,2048]{1,0:T(8,128)(2,1)} %stream_ref.1, f32[1,2048]{1,0:T(1,128)} %bitcast.11, s32[4,128]{1,0:T(4,128)} %bitcast.13, f32[4,128]{1,0:T(4,128)} %bitcast.14, bf16[1024,2048]{1,0:T(8,128)(2,1)} %out_weight_hbm.1, ...), custom_call_target="tpu_custom_call" | custom-call | tf_op jit(solution)/shard_map/pallas_call | solution.py:528
  133.0 1.9 %copy.26 = bf16[128,2048]{1,0:T(8,128)(2,1)} copy(bf16[128,2048]{1,0:T(8,128)(2,1)} %shard_map.227) | data formatting | bytes 1048576

commit v4 on v3

--- a/solution.py
+++ b/solution.py
@@ -13,23 +13,37 @@
 
 MESH = pl.DeviceIdType.MESH
 PLANES = 4
+HALVES = 2
 COLS = 512
 
 
-LINE_END = [(0, 0), (0, 1), (3, 0), (0, 2), (1, 1), (1, 2), (0, 3), (2, 2), (2, 1), (1, 3), (2, 3), (1, 0), (2, 0)]
-LINE_NEXT = [(0, 1), (0, 2), (0, 0), (3, 0), (1, 2), (0, 3), (2, 2), (1, 0), (1, 3), (2, 0), (2, 3), (1, 1), (2, 1)]
-
-
-def line_plans(planes):
-    if planes == 4:
-        mirror = lambda plan: [(kind, 3 - owner) for kind, owner in plan]
+LINE_END = [
+    (0, 0, 0), (0, 0, 1), (0, 1, 0), (1, 0, 0), (0, 2, 0), (0, 2, 1),
+    (0, 3, 0), (1, 2, 0), (2, 2, 0), (0, 3, 1), (0, 1, 1), (2, 2, 1),
+    (1, 3, 0), (2, 3, 0), (1, 1, 0), (3, 0, 0), (2, 3, 1), (2, 0, 0),
+    (2, 1, 0), (2, 1, 1), (2, 0, 1),
+]
+LINE_NEXT = [
+    (0, 1, 0), (0, 1, 1), (0, 0, 0), (0, 2, 0), (0, 2, 1), (0, 3, 0),
+    (1, 2, 0), (0, 0, 1), (2, 2, 0), (0, 3, 1), (2, 2, 1), (1, 0, 0),
+    (2, 0, 0), (1, 3, 0), (1, 1, 0), (2, 0, 1), (2, 3, 0), (3, 1, 0),
+    (2, 1, 0), (2, 1, 1), (2, 3, 1),
+]
+
+
+def line_plans(planes, halves):
+    if (planes, halves) == (4, 2):
+        mirror = lambda plan: [(kind, 3 - owner, half) for kind, owner, half in plan]
         plans = [LINE_END, LINE_NEXT, mirror(LINE_NEXT), mirror(LINE_END)]
     else:
         plans = []
         for z in range(planes):
             near = sorted(range(planes), key=lambda s: (abs(s - z), s))
-            plans.append([(0, s) for s in near] + [(3, 0)] + [(k, s) for s in near for k in (1, 2)])
-    return [[kind * planes + owner for kind, owner in plan] for plan in plans]
+            plan = [(0, s, h) for s in near for h in range(halves)] + [(3, 0, 0)]
+            for s in near:
+                plan += [(1, s, 0)] + [(2, s, h) for h in range(halves)]
+            plans.append(plan)
+    return [[(k * planes + s) * halves + h for k, s, h in plan] for plan in plans]
 
 
 def column_chunks(width):
@@ -51,12 +65,13 @@
     return chosen
 
 
-def tail_kernel(
+def tail_stage(
     planes,
     ring,
     tp_count,
     capacity,
     fanout,
+    mix,
     mixed_ref,
     stream_ref,
     gain_ref,
@@ -83,6 +98,7 @@
     residual,
     part_out,
     part_in,
+    normed,
     rows,
     sent,
     arrived,
@@ -90,6 +106,7 @@
     hidden,
     answer,
     returned,
+    sums_own,
     sums_out,
     sums_in,
     weight_sem,
@@ -112,8 +129,10 @@
     chips = ring // tp_count
     plane = chip // chips
     mine = (chip % chips) * tp_count + core
-    count, width = rows.shape[1], rows.shape[2]
-    plans = line_plans(planes)
+    count, width = stream_ref.shape
+    halves = rows.shape[1]
+    part = width // halves
+    plans = line_plans(planes, halves)
 
     def in_plane(spot):
         return (plane * chips + spot // tp_count, spot % tp_count)
@@ -139,15 +158,20 @@
         load.start()
 
     barrier = pltpu.get_barrier_semaphore()
-    for ahead in range(1, ring):
+    all_chips = lax.axis_size("sp")
+    for ahead in range(1, all_chips):
         pl.semaphore_signal(
-            barrier, inc=1, device_id=in_plane((mine + ahead) % ring), device_id_type=MESH
-        )
-    for ahead in range(1, planes):
-        pl.semaphore_signal(
-            barrier, inc=1, device_id=in_line((plane + ahead) % planes), device_id_type=MESH
-        )
-    pl.semaphore_wait(barrier, ring + planes - 2)
+            barrier, inc=1, device_id=((chip + ahead) % all_chips, core), device_id_type=MESH
+        )
+    for spot in range(chips):
+        for ahead in range(1, tp_count):
+            pl.semaphore_signal(
+                barrier,
+                inc=1,
+                device_id=(plane * chips + spot, (core + ahead) % tp_count),
+                device_id_type=MESH,
+            )
+    pl.semaphore_wait(barrier, all_chips - 1 + chips * (tp_count - 1))
 
     def table_copies(ahead, owner):
         return [
@@ -169,33 +193,39 @@
             copy.start()
     index_tables[plane] = index_ref[...]
     weight_tables[plane] = weight_ref[...]
-
-    def part_copy(ahead):
-        return pltpu.make_async_remote_copy(
-            src_ref=part_out.at[ahead - 1],
-            dst_ref=part_in.at[ahead - 1],
-            send_sem=part_send.at[ahead - 1],
-            recv_sem=part_recv.at[ahead - 1],
-            device_id=(chip, (core + ahead) % tp_count),
-            device_id_type=MESH,
-        )
+    mix()
+
+    def part_copies(ahead):
+        return [
+            pltpu.make_async_remote_copy(
+                src_ref=part_out.at[ahead - 1, :, pl.ds(at, step)],
+                dst_ref=part_in.at[ahead - 1, :, pl.ds(at, step)],
+                send_sem=part_send.at[ahead - 1, number],
+                recv_sem=part_recv.at[ahead - 1, number],
+                device_id=(chip, (core + ahead) % tp_count),
+                device_id_type=MESH,
+            )
+            for number, (at, step) in enumerate(column_chunks(width))
+        ]
 
     loads[0].wait()
     for ahead in range(1, tp_count):
         owner = (core + ahead) % tp_count
         held = mixed_ref[pl.ds(pl.multiple_of(owner * count, count), count), :]
-        for at, step in column_chunks(width):
+        copies = part_copies(ahead)
+        for number, (at, step) in enumerate(column_chunks(width)):
             part_out[ahead - 1, :, at : at + step] = jnp.dot(
                 held, out_weight[:, at : at + step], preferred_element_type=jnp.float32
             ).astype(jnp.bfloat16)
-        part_copy(ahead).start()
+            copies[number].start()
     held = mixed_ref[pl.ds(pl.multiple_of(core * count, count), count), :]
     for at, step in column_chunks(width):
         total[:, at : at + step] = stream_ref[:, at : at + step].astype(jnp.float32) + jnp.dot(
             held, out_weight[:, at : at + step], preferred_element_type=jnp.float32
         )
     for ahead in range(1, tp_count):
-        part_copy(ahead).wait_recv()
+        for copy in part_copies(ahead):
+            copy.wait_recv()
     band = 16
 
     def norm_band(number, carry):
@@ -207,81 +237,64 @@
         wide = rounded.astype(jnp.float32)
         total[spot, :] = wide
         scale = lax.rsqrt(jnp.mean(wide * wide, axis=-1, keepdims=True) + 1e-06)
-        rows[plane, spot, :] = (wide * scale * gain_ref[...]).astype(jnp.bfloat16)
+        value = (wide * scale * gain_ref[...]).astype(jnp.bfloat16)
+        normed[spot, :] = value
+        for half in range(halves):
+            rows[plane, half, spot, :] = value[:, half * part : (half + 1) * part]
         return carry
 
     lax.fori_loop(0, count // band, norm_band, 0)
 
-    def rows_copy(owner, target, sem):
+    def rows_copy(owner, half, target, sem):
         return pltpu.make_async_remote_copy(
-            src_ref=rows.at[owner],
-            dst_ref=rows.at[owner],
-            send_sem=sem.at[owner],
-            recv_sem=rows_recv.at[owner],
+            src_ref=rows.at[owner, half],
+            dst_ref=rows.at[owner, half],
+            send_sem=sem.at[owner, half],
+            recv_sem=rows_recv.at[owner, half],
             device_id=in_line(target),
             device_id_type=MESH,
         )
 
-    def go_copy(owner, ahead):
+    def block_copy(source, target, send, recv, owner, half, ahead):
         spot = (mine + ahead) % ring
         return pltpu.make_async_remote_copy(
-            src_ref=sent.at[owner, spot],
-            dst_ref=arrived.at[owner, mine],
-            send_sem=go_send.at[owner, spot],
-            recv_sem=go_recv.at[owner, mine],
+            src_ref=source.at[owner, half, spot],
+            dst_ref=target.at[owner, half, mine],
+            send_sem=send.at[owner, half],
+            recv_sem=recv.at[owner, half],
             device_id=in_plane(spot),
             device_id_type=MESH,
         )
 
-    def go_wait(owner, ahead):
-        spot = (mine + ahead) % ring
+    def block_wait(source, target, send, recv, owner, half):
         return pltpu.make_async_remote_copy(
-            src_ref=sent.at[owner, spot],
-            dst_ref=arrived.at[owner, spot],
-            send_sem=go_send.at[owner, spot],
-            recv_sem=go_recv.at[owner, spot],
-            device_id=in_plane(spot),
+            src_ref=source.at[owner, half, pl.ds(0, ring - 1)],
+            dst_ref=target.at[owner, half, pl.ds(0, ring - 1)],
+            send_sem=send.at[owner, half],
+            recv_sem=recv.at[owner, half],
+            device_id=in_plane((mine + 1) % ring),
             device_id_type=MESH,
         )
 
-    def back_copy(owner, ahead):
-        spot = (mine + ahead) % ring
+    go = (sent, arrived, go_send, go_recv)
+    back = (answer, returned, back_send, back_recv)
+
+    def sums_copy(owner, half):
         return pltpu.make_async_remote_copy(
-            src_ref=answer.at[owner, spot],
-            dst_ref=returned.at[owner, mine],
-            send_sem=back_send.at[owner, spot],
-            recv_sem=back_recv.at[owner, mine],
-            device_id=in_plane(spot),
-            device_id_type=MESH,
-        )
-
-    def back_wait(owner, ahead):
-        spot = (mine + ahead) % ring
-        return pltpu.make_async_remote_copy(
-            src_ref=answer.at[owner, spot],
-            dst_ref=returned.at[owner, spot],
-            send_sem=back_send.at[owner, spot],
-            recv_sem=back_recv.at[owner, spot],
-            device_id=in_plane(spot),
-            device_id_type=MESH,
-        )
-
-    def sums_copy(owner):
-        return pltpu.make_async_remote_copy(
-            src_ref=sums_out.at[owner],
-            dst_ref=sums_in.at[plane],
-            send_sem=sums_send.at[owner],
-            recv_sem=sums_recv.at[plane],
+            src_ref=sums_out.at[owner, half],
+            dst_ref=sums_in.at[plane, half],
+            send_sem=sums_send.at[owner, half],
+            recv_sem=sums_recv.at[plane, half],
             device_id=in_line(owner),
             device_id_type=MESH,
         )
 
-    def sums_wait(owner):
+    def sums_wait(owner, half):
         return pltpu.make_async_remote_copy(
-            src_ref=sums_out.at[owner],
-            dst_ref=sums_in.at[owner],
-            send_sem=sums_send.at[owner],
-            recv_sem=sums_recv.at[owner],
+            src_ref=sums_out.at[owner, half],
+            dst_ref=sums_in.at[owner, half],
+            send_sem=sums_send.at[owner, half],
+            recv_sem=sums_recv.at[owner, half],
             device_id=in_line(owner),
             device_id_type=MESH,
         )
@@ -308,19 +321,22 @@
         for copy in table_copies(ahead, owner):
             copy.wait_recv()
 
-    def dispatch(owner):
+    def dispatch(owner, half):
         @pl.when(owner != plane)
         def _():
-            rows_copy(owner, owner, rows_up).wait_recv()
+            rows_copy(owner, half, owner, rows_up).wait_recv()
+
+        @pl.when((owner <= plane) & (plane < planes - 1))
+        def _():
+            rows_copy(owner, half, plane + 1, rows_up).start()
+
+        @pl.when((owner >= plane) & (plane > 0))
+        def _():
+            rows_copy(owner, half, plane - 1, rows_down).start()
+
+        @pl.when((owner != plane) & (half == 0))
+        def _():
             wait_table(owner)
-
-        @pl.when((owner <= plane) & (plane < planes - 1))
-        def _():
-            rows_copy(owner, plane + 1, rows_up).start()
-
-        @pl.when((owner >= plane) & (plane > 0))
-        def _():
-            rows_copy(owner, plane - 1, rows_down).start()
 
         slot, _ = slots_of(owner)
         chosen = jnp.concatenate(
@@ -330,17 +346,17 @@
             ],
             axis=0,
         ).astype(jnp.bfloat16)
-        for at, step in column_chunks(width):
+        for at, step in column_chunks(part):
             picked = jnp.dot(
-                chosen, rows[owner, :, at : at + step], preferred_element_type=jnp.float32
+                chosen, rows[owner, half, :, at : at + step], preferred_element_type=jnp.float32
             )
             for spot in range(ring):
-                sent[owner, spot, :, at : at + step] = picked[
+                sent[owner, half, spot, :, at : at + step] = picked[
                     spot * capacity : (spot + 1) * capacity
                 ].astype(jnp.bfloat16)
         for ahead in range(1, ring):
-            go_copy(owner, ahead).start()
-        arrived[owner, mine] = sent[owner, mine]
+            block_copy(*go, owner, half, ahead).start()
+        arrived[owner, half, mine] = sent[owner, half, mine]
 
     def ffn(x_ref, gate_ref, up_ref, down_ref, hidden_ref, put):
         for at, step in column_chunks(gate_ref.shape[1]):
@@ -365,31 +381,33 @@
             )
 
     def serve(owner):
-        for ahead in range(1, ring):
-            go_wait(owner, ahead).wait_recv()
-        for at, step in column_chunks(width):
-            flat[:, at : at + step] = jnp.concatenate(
-                [
-                    arrived[owner, spot, :, at : at + step].astype(jnp.float32)
-                    for spot in range(ring)
-                ],
-                axis=0,
-            ).astype(jnp.bfloat16)
+        for half in range(halves):
+            block_wait(*go, owner, half).wait_recv()
+            for at, step in column_chunks(part):
+                flat[:, half * part + at : half * part + at + step] = jnp.concatenate(
+                    [
+                        arrived[owner, half, spot, :, at : at + step].astype(jnp.float32)
+                        for spot in range(ring)
+                    ],
+                    axis=0,
+                ).astype(jnp.bfloat16)
 
         def put(at, step, value):
+            half, lane = at // part, at % part
             for spot in range(ring):
-                answer[owner, spot, :, at : at + step] = value[
+                answer[owner, half, spot, :, lane : lane + step] = value[
                     spot * capacity : (spot + 1) * capacity
                 ].astype(jnp.bfloat16)
+            if lane + step == part:
+                for ahead in range(1, ring):
+                    block_copy(*back, owner, half, ahead).start()
 
         ffn(flat, gate, up, down, hidden, put)
-        for ahead in range(1, ring):
-            back_copy(owner, ahead).start()
-        returned[owner, mine] = answer[owner, mine]
-
-    def collect(owner):
-        for ahead in range(1, ring):
-            back_wait(owner, ahead).wait_recv()
+        for half in range(halves):
+            returned[owner, half, mine] = answer[owner, half, mine]
+
+    def collect(owner, half):
+        block_wait(*back, owner, half).wait_recv()
         slot, share = slots_of(owner)
         spread = jnp.concatenate(
             [
@@ -401,30 +419,30 @@
         coarse = spread.astype(jnp.bfloat16)
         fine = (spread - coarse.astype(jnp.float32)).astype(jnp.bfloat16)
         contract = (((0,), (0,)), ((), ()))
-        for at, step in column_chunks(width):
-            back = jnp.concatenate(
+        for at, step in column_chunks(part):
+            blocks = jnp.concatenate(
                 [
-                    returned[owner, spot, :, at : at + step].astype(jnp.float32)
+                    returned[owner, half, spot, :, at : at + step].astype(jnp.float32)
                     for spot in range(ring)
                 ],
                 axis=0,
             ).astype(jnp.bfloat16)
-            value = lax.dot_general(coarse, back, contract, preferred_element_type=jnp.float32)
+            value = lax.dot_general(coarse, blocks, contract, preferred_element_type=jnp.float32)
             value = value + lax.dot_general(
-                fine, back, contract, preferred_element_type=jnp.float32
+                fine, blocks, contract, preferred_element_type=jnp.float32
             )
 
             @pl.when(owner == plane)
             def _():
-                total[:, at : at + step] += value
+                sums_own[half, :, at : at + step] = value
 
             @pl.when(owner != plane)
             def _():
-                sums_out[owner, :, at : at + step] = value.astype(jnp.bfloat16)
+                sums_out[owner, half, :, at : at + step] = value.astype(jnp.bfloat16)
 
         @pl.when(owner != plane)
         def _():
-            sums_copy(owner).start()
+            sums_copy(owner, half).start()
 
     def share_expert():
         for load in loads[1:4]:
@@ -433,15 +451,15 @@
         def put(at, step, value):
             total[:, at : at + step] += value
 
-        ffn(rows.at[plane], common_gate, common_up, common_down, residual, put)
+        ffn(normed, common_gate, common_up, common_down, residual, put)
 
     def step(turn, carry):
         code = pick(plans, plane, turn)
-        kind, owner = code // planes, code % planes
+        half, owner, kind = code % halves, code // halves % planes, code // (halves * planes)
 
         @pl.when(kind == 0)
         def _():
-            dispatch(owner)
+            dispatch(owner, half)
 
         @pl.when(kind == 1)
         def _():
@@ -449,7 +467,7 @@
 
         @pl.when(kind == 2)
         def _():
-            collect(owner)
+            collect(owner, half)
 
         @pl.when(kind == 3)
         def _():
@@ -462,129 +480,50 @@
     lax.fori_loop(0, len(plans[0]), step, 0)
 
     for ahead in range(1, planes):
-        sums_wait((plane + ahead) % planes).wait_recv()
+        for half in range(halves):
+            sums_wait((plane + ahead) % planes, half).wait_recv()
 
     def last_band(number, carry):
         spot = pl.ds(pl.multiple_of(number * band, band), band)
-        summed = total[spot, :]
-        for ahead in range(1, planes):
-            summed = summed + sums_in[(plane + ahead) % planes, spot, :].astype(jnp.float32)
-        out_ref[spot, :] = summed.astype(jnp.bfloat16)
+        for half in range(halves):
+            lanes = slice(half * part, (half + 1) * part)
+            value = total[spot, lanes] + sums_own[half, spot, :]
+            for ahead in range(1, planes):
+                value = value + sums_in[(plane + ahead) % planes, half, spot, :].astype(
+                    jnp.float32
+                )
+            out_ref[spot, lanes] = value.astype(jnp.bfloat16)
         return carry
 
     lax.fori_loop(0, count // band, last_band, 0)
 
     for ahead in range(1, tp_count):
-        part_copy(ahead).wait_send()
+        for copy in part_copies(ahead):
+            copy.wait_send()
     for ahead in range(1, planes):
         for copy in table_copies(ahead, plane):
             copy.wait_send()
-        sums_copy((plane + ahead) % planes).wait_send()
-    for owner in range(planes):
+
+    def drain(code, carry):
+        owner, half = code // halves, code % halves
+        block_wait(*go, owner, half).wait_send()
+        block_wait(*back, owner, half).wait_send()
+
+        @pl.when(owner != plane)
+        def _():
+            sums_copy(owner, half).wait_send()
 
         @pl.when((owner <= plane) & (plane < planes - 1))
         def _():
-            rows_copy(owner, plane + 1, rows_up).wait_send()
+            rows_copy(owner, half, plane + 1, rows_up).wait_send()
 
         @pl.when((owner >= plane) & (plane > 0))
         def _():
-            rows_copy(owner, plane - 1, rows_down).wait_send()
-
-    def drain(owner, carry):
-        for ahead in range(1, ring):
-            go_copy(owner, ahead).wait_send()
-            back_copy(owner, ahead).wait_send()
+            rows_copy(owner, half, plane - 1, rows_down).wait_send()
+
         return carry
 
-    lax.fori_loop(0, planes, drain, 0)
-
-
-def tail(
-    mixed,
-    stream,
-    gain,
-    index,
-    weight,
-    out_weight,
-    gate,
-    up,
-    down,
-    common_gate,
-    common_up,
-    common_down,
-):
-    sp_count, tp_count = lax.axis_size("sp"), lax.axis_size("tp")
-    planes = PLANES if sp_count % PLANES == 0 else 1
-    ring = sp_count // planes * tp_count
-    count, width = stream.shape
-    fanout = index.shape[1]
-    experts = sp_count * tp_count
-    capacity = max(2, (3 * count * fanout + 2 * experts - 1) // (2 * experts))
-    capacity = (capacity + 7) // 8 * 8
-    bf16 = jnp.bfloat16
-    vmem, anywhere = pl.BlockSpec(memory_space=pltpu.VMEM), pl.BlockSpec(memory_space=pl.ANY)
-    slots = (planes, ring, capacity, width)
-    dma = pltpu.SemaphoreType.DMA
-    return pl.pallas_call(
-        functools.partial(tail_kernel, planes, ring, tp_count, capacity, fanout),
-        out_shape=jax.ShapeDtypeStruct((count, width), bf16),
-        in_specs=[vmem] * 5 + [anywhere] * 7,
-        out_specs=vmem,
-        scratch_shapes=[
-            pltpu.VMEM(out_weight.shape, bf16),
-            pltpu.VMEM(gate.shape[1:], bf16),
-            pltpu.VMEM(up.shape[1:], bf16),
-            pltpu.VMEM(down.shape[1:], bf16),
-            pltpu.VMEM(common_gate.shape, bf16),
-            pltpu.VMEM(common_up.shape, bf16),
-            pltpu.VMEM(common_down.shape, bf16),
-            pltpu.VMEM((planes, fanout, count), jnp.int32),
-            pltpu.VMEM((planes, fanout, count), jnp.float32),
-            pltpu.VMEM((count, width), jnp.float32),
-            pltpu.VMEM((count, common_gate.shape[1]), bf16),
-            pltpu.VMEM((tp_count - 1, count, width), bf16),
-            pltpu.VMEM((tp_count - 1, count, width), bf16),
-            pltpu.VMEM((planes, count, width), bf16),
-            pltpu.VMEM(slots, bf16),
-            pltpu.VMEM(slots, bf16),
-            pltpu.VMEM((ring * capacity, width), bf16),
-            pltpu.VMEM((ring * capacity, gate.shape[2]), bf16),
-            pltpu.VMEM(slots, bf16),
-            pltpu.VMEM(slots, bf16),
-            pltpu.VMEM((planes, count, width), bf16),
-            pltpu.VMEM((planes, count, width), bf16),
-            dma((7,)),
-            dma((tp_count - 1,)),
-            dma((tp_count - 1,)),
-            dma((2, planes)),
-            dma((2, planes)),
-            dma((planes,)),
-            dma((planes,)),
-            dma((planes,)),
-            dma((planes, ring)),
-            dma((planes, ring)),
-            dma((planes, ring)),
-            dma((planes, ring)),
-            dma((planes,)),
-            dma((planes,)),
-        ],
-        compiler_params=pltpu.CompilerParams(
-            collective_id=0, has_side_effects=True, vmem_limit_bytes=60 * 2**20
-        ),
-    )(
-        mixed,
-        stream,
-        gain.reshape(1, -1),
-        index.T,
-        weight.T,
-        out_weight,
-        gate,
-        up,
-        down,
-        common_gate,
-        common_up,
-        common_down,
-    )
+    lax.fori_loop(0, planes * halves, drain, 0)
 
 
 def mixer_stage(
@@ -936,63 +875,89 @@
     ]
 
 
-def mixer_kernel(heads, groups, owners, head_dim, *refs):
-    chip, core = lax.axis_index("sp"), lax.axis_index("tp")
-    chips = lax.axis_size("sp")
-    barrier = pltpu.get_barrier_semaphore()
-    for ahead in range(1, chips):
-        pl.semaphore_signal(
-            barrier, inc=1, device_id=((chip + ahead) % chips, core), device_id_type=MESH
-        )
-    pl.semaphore_wait(barrier, chips - 1)
-    mixer_stage(heads, groups, owners, head_dim, *refs)
-
-
-def mixer(
-    signal_in,
-    write_in,
-    read_in,
-    gate_in,
-    step_in,
-    log_in,
-    signal_taps,
-    write_taps,
-    read_taps,
-    bias,
-    rate,
-    direct,
-    gain,
-):
-    chips = lax.axis_size("sp")
-    length, wide = signal_in.shape
-    narrow = write_in.shape[1]
-    heads = step_in.shape[1]
-    owners = min(chips, STATE // 8)
-    vmem = pl.BlockSpec(memory_space=pltpu.VMEM)
+def layer_kernel(tail_sizes, mixer_sizes, mixer_scratch_count, *refs):
+    mixer_in, tail_in, out = refs[:13], refs[13:24], refs[24]
+    mixed = refs[25]
+    mixer_refs = refs[26 : 26 + mixer_scratch_count]
+    tail_refs = refs[26 + mixer_scratch_count :]
+
+    def mix():
+        mixer_stage(*mixer_sizes, *mixer_in, mixed, *mixer_refs)
+
+    tail_stage(*tail_sizes, mix, mixed, *tail_in, out, *tail_refs)
+
+
+def layer(mixer_in, tail_in):
+    sp_count, tp_count = lax.axis_size("sp"), lax.axis_size("tp")
+    bf16, f32 = jnp.bfloat16, jnp.float32
+    dma = pltpu.SemaphoreType.DMA
+    vmem, anywhere = pl.BlockSpec(memory_space=pltpu.VMEM), pl.BlockSpec(memory_space=pl.ANY)
+    length, wide = mixer_in[0].shape
+    narrow = mixer_in[1].shape[1]
+    heads = mixer_in[4].shape[0]
+    owners = min(sp_count, STATE // 8)
+    mixer_sizes = (heads, narrow // STATE, owners, wide // heads)
+    mixer_refs = mixer_scratch(sp_count, owners, length, wide, narrow, length // BLK)
+    stream, _, index, _, out_weight, gate, up, down, common_gate, common_up, common_down = tail_in
+    planes = PLANES if sp_count % PLANES == 0 else 1
+    ring = sp_count // planes * tp_count
+    count, width = stream.shape
+    fanout = index.shape[0]
+    experts = sp_count * tp_count
+    capacity = max(2, (3 * count * fanout + 2 * experts - 1) // (2 * experts))
+    capacity = (capacity + 7) // 8 * 8
+    part = width // HALVES
+    chunks = len(column_chunks(width))
+    slots = (planes, HALVES, ring, capacity, part)
+    pieces = (planes, HALVES, count, part)
     return pl.pallas_call(
-        functools.partial(mixer_kernel, heads, narrow // STATE, owners, wide // heads),
-        out_shape=jax.ShapeDtypeStruct((length, wide), jnp.bfloat16),
-        in_specs=[vmem] * 13,
+        functools.partial(
+            layer_kernel,
+            (planes, ring, tp_count, capacity, fanout),
+            mixer_sizes,
+            len(mixer_refs),
+        ),
+        out_shape=jax.ShapeDtypeStruct((count, width), bf16),
+        in_specs=[vmem] * 17 + [anywhere] * 7,
         out_specs=vmem,
-        scratch_shapes=mixer_scratch(chips, owners, length, wide, narrow, length // BLK),
+        scratch_shapes=[
+            pltpu.VMEM((length, wide), bf16),
+            *mixer_refs,
+            pltpu.VMEM(out_weight.shape, bf16),
+            pltpu.VMEM(gate.shape[1:], bf16),
+            pltpu.VMEM(up.shape[1:], bf16),
+            pltpu.VMEM(down.shape[1:], bf16),
+            pltpu.VMEM(common_gate.shape, bf16),
+            pltpu.VMEM(common_up.shape, bf16),
+            pltpu.VMEM(common_down.shape, bf16),
+            pltpu.VMEM((planes, fanout, count), jnp.int32),
+            pltpu.VMEM((planes, fanout, count), f32),
+            pltpu.VMEM((count, width), f32),
+            pltpu.VMEM((count, common_gate.shape[1]), bf16),
+            pltpu.VMEM((tp_count - 1, count, width), bf16),
+            pltpu.VMEM((tp_count - 1, count, width), bf16),
+            pltpu.VMEM((count, width), bf16),
+            pltpu.VMEM(pieces, bf16),
+            pltpu.VMEM(slots, bf16),
+            pltpu.VMEM(slots, bf16),
+            pltpu.VMEM((ring * capacity, width), bf16),
+            pltpu.VMEM((ring * capacity, gate.shape[2]), bf16),
+            pltpu.VMEM(slots, bf16),
+            pltpu.VMEM(slots, bf16),
+            pltpu.VMEM(pieces[1:], f32),
+            pltpu.VMEM(pieces, bf16),
+            pltpu.VMEM(pieces, bf16),
+            dma((7,)),
+            dma((tp_count - 1, chunks)),
+            dma((tp_count - 1, chunks)),
+            dma((2, planes)),
+            dma((2, planes)),
+            *[dma((planes, HALVES))] * 9,
+        ],
         compiler_params=pltpu.CompilerParams(
-            collective_id=1, has_side_effects=True, vmem_limit_bytes=60 * 2**20
+            collective_id=0, has_side_effects=True, vmem_limit_bytes=62 * 2**20
         ),
-    )(
-        signal_in,
-        write_in,
-        read_in,
-        gate_in,
-        step_in.T,
-        log_in.T,
-        signal_taps,
-        write_taps,
-        read_taps,
-        bias.reshape(1, -1),
-        rate.reshape(1, -1),
-        direct.reshape(1, -1),
-        gain.reshape(1, -1),
-    )
+    )(*mixer_in, *tail_in)
 
 
 def on_device(
@@ -1021,34 +986,36 @@
     common_up_weight,
     common_down_weight,
 ):
-    mixer_out = mixer(
-        head_input_signal,
-        write_input_vectors,
-        read_input_vectors,
-        output_gate_input,
-        step_size_input,
-        position_log_decay,
-        signal_filter_taps,
-        write_filter_taps,
-        read_filter_taps,
-        step_size_bias,
-        head_decay_rate,
-        head_direct_term,
-        grouped_norm_gain,
-    )
-    return tail(
-        mixer_out,
-        stream,
-        expert_norm_gain,
-        chosen_expert_index,
-        chosen_expert_weight,
-        mixer_output_weight,
-        routed_gate_weight,
-        routed_up_weight,
-        routed_down_weight,
-        common_gate_weight,
-        common_up_weight,
-        common_down_weight,
+    row = lambda part: part.reshape(1, -1)
+    return layer(
+        (
+            head_input_signal,
+            write_input_vectors,
+            read_input_vectors,
+            output_gate_input,
+            step_size_input.T,
+            position_log_decay.T,
+            signal_filter_taps,
+            write_filter_taps,
+            read_filter_taps,
+            row(step_size_bias),
+            row(head_decay_rate),
+            row(head_direct_term),
+            row(grouped_norm_gain),
+        ),
+        (
+            stream,
+            row(expert_norm_gain),
+            chosen_expert_index.T,
+            chosen_expert_weight.T,
+            mixer_output_weight,
+            routed_gate_weight,
+            routed_up_weight,
+            routed_down_weight,
+            common_gate_weight,
+            common_up_weight,
+            common_down_weight,
+        ),
     )
 
 

time: 136 us -> 121 us (0.89)
  Pallas kernels: 133 us -> 119 us
    pallas_call x2 -> x1, Pallas kernels: 133 us -> 119 us  [layer(): pl.pallas_call(functools.partial(layer_kernel, (planes, ring, tp_count, c...]
where the time goes in v4:
time: 121 us
  Pallas kernels  119 us (98%)
  local copies, waits for them, and re-layouts  1.88 us (2%)
    pallas_call x1, Pallas kernels, layer(): pl.pallas_call(functools.partial(layer_kernel, (planes, ring, tp_count, c...  119 us

profile of v4, /device:TPU:0, one launch (start us, length us, event | category | flops | bytes accessed | tf_op | source)
XLA Modules:
  0.0 120.8 jit_solution(11763342218244561566)
XLA Ops:
  0.0 119.0 %shard_map.226 = bf16[128,2048]{1,0:T(8,128)(2,1)} custom-call(bf16[256,1024]{1,0:T(8,128)(2,1)} %refs_0_.1, bf16[256,256]{1,0:T(8,128)(2,1)} %refs_1_.1, bf16[256,256]{1,0:T(8,128)(2,1)} %refs_2_.1, bf16[256,1024]{1,0:T(8,128)(2,1)} %refs_3_.1, bf16[16,256]{1,0:T(8,128)(2,1)} %bitcast.10, f32[16,256]{1,0:T(8,128)} %bitcast.9, bf16[4,1024]{1,0:T(4,128)(2,1)} %refs_6_.1, ...), custom_call_target="tpu_custom_call" | custom-call | tf_op jit(solution)/shard_map/pallas_call | solution.py:913
  119.0 1.9 %copy.26 = bf16[128,2048]{1,0:T(8,128)(2,1)} copy(bf16[128,2048]{1,0:T(8,128)(2,1)} %shard_map.226) | data formatting | bytes 1048576

commit v5 on v4

--- a/solution.py
+++ b/solution.py
@@ -18,16 +18,16 @@
 
 
 LINE_END = [
-    (0, 0, 0), (0, 0, 1), (0, 1, 0), (1, 0, 0), (0, 2, 0), (0, 2, 1),
-    (0, 3, 0), (1, 2, 0), (2, 2, 0), (0, 3, 1), (0, 1, 1), (2, 2, 1),
-    (1, 3, 0), (2, 3, 0), (1, 1, 0), (3, 0, 0), (2, 3, 1), (2, 0, 0),
-    (2, 1, 0), (2, 1, 1), (2, 0, 1),
+    (0, 0, 0), (0, 0, 1), (0, 1, 0), (0, 1, 1), (0, 2, 0), (0, 2, 1),
+    (0, 3, 0), (1, 2, 0), (2, 2, 0), (0, 3, 1), (2, 2, 1), (3, 0, 0),
+    (1, 3, 0), (2, 3, 0), (1, 1, 0), (1, 0, 0), (2, 3, 1), (2, 1, 0),
+    (2, 1, 1), (2, 0, 0), (2, 0, 1),
 ]
 LINE_NEXT = [
-    (0, 1, 0), (0, 1, 1), (0, 0, 0), (0, 2, 0), (0, 2, 1), (0, 3, 0),
-    (1, 2, 0), (0, 0, 1), (2, 2, 0), (0, 3, 1), (2, 2, 1), (1, 0, 0),
-    (2, 0, 0), (1, 3, 0), (1, 1, 0), (2, 0, 1), (2, 3, 0), (3, 1, 0),
-    (2, 1, 0), (2, 1, 1), (2, 3, 1),
+    (0, 1, 0), (0, 1, 1), (3, 1, 0), (0, 0, 0), (0, 2, 0), (0, 2, 1),
+    (0, 3, 0), (0, 0, 1), (1, 2, 0), (1, 0, 0), (0, 3, 1), (1, 1, 0),
+    (2, 0, 0), (2, 2, 0), (1, 3, 0), (2, 1, 0), (2, 2, 1), (2, 0, 1),
+    (2, 3, 0), (2, 3, 1), (2, 1, 1),
 ]
 
 
@@ -63,6 +63,18 @@
     for spot, value in enumerate(row):
         chosen = chosen + (which == spot).astype(jnp.int32) * value
     return chosen
+
+
+def bytes_of(ref, number, send_sem, recv_sem):
+    view = ref.at[pl.ds(0, number)]
+    return pltpu.make_async_remote_copy(
+        src_ref=view,
+        dst_ref=view,
+        send_sem=send_sem,
+        recv_sem=recv_sem,
+        device_id=(lax.axis_index("sp"), lax.axis_index("tp")),
+        device_id_type=MESH,
+    )
 
 
 def tail_stage(
@@ -109,6 +121,7 @@
     sums_own,
     sums_out,
     sums_in,
+    relay_in,
     weight_sem,
     part_send,
     part_recv,
@@ -123,6 +136,7 @@
     back_recv,
     sums_send,
     sums_recv,
+    relay_recv,
 ):
     chip = lax.axis_index("sp")
     core = lax.axis_index("tp")
@@ -178,8 +192,8 @@
             pltpu.make_async_remote_copy(
                 src_ref=source,
                 dst_ref=held.at[owner],
-                send_sem=table_send.at[number, ahead],
-                recv_sem=table_recv.at[number, owner],
+                send_sem=table_send.at[number],
+                recv_sem=table_recv.at[number],
                 device_id=in_line((plane + ahead) % planes),
                 device_id_type=MESH,
             )
@@ -193,14 +207,32 @@
             copy.start()
     index_tables[plane] = index_ref[...]
     weight_tables[plane] = weight_ref[...]
+    relayed = planes == 4
+    if relayed:
+
+        @pl.when(plane == 0)
+        def _():
+            sums_in[planes - 1] = jnp.zeros(sums_in.shape[1:], jnp.bfloat16)
+
+        @pl.when(plane == planes - 1)
+        def _():
+            sums_in[0] = jnp.zeros(sums_in.shape[1:], jnp.bfloat16)
+
     mix()
+    table_totals = [
+        bytes_of(held, planes - 1, table_send.at[number], table_recv.at[number])
+        for number, held in enumerate([index_tables, weight_tables])
+    ]
+    if planes > 1:
+        for total_copy in table_totals:
+            total_copy.wait_recv()
 
     def part_copies(ahead):
         return [
             pltpu.make_async_remote_copy(
                 src_ref=part_out.at[ahead - 1, :, pl.ds(at, step)],
                 dst_ref=part_in.at[ahead - 1, :, pl.ds(at, step)],
-                send_sem=part_send.at[ahead - 1, number],
+                send_sem=part_send.at[ahead - 1],
                 recv_sem=part_recv.at[ahead - 1, number],
                 device_id=(chip, (core + ahead) % tp_count),
                 device_id_type=MESH,
@@ -260,7 +292,7 @@
         return pltpu.make_async_remote_copy(
             src_ref=source.at[owner, half, spot],
             dst_ref=target.at[owner, half, mine],
-            send_sem=send.at[owner, half],
+            send_sem=send.at[0],
             recv_sem=recv.at[owner, half],
             device_id=in_plane(spot),
             device_id_type=MESH,
@@ -270,7 +302,7 @@
         return pltpu.make_async_remote_copy(
             src_ref=source.at[owner, half, pl.ds(0, ring - 1)],
             dst_ref=target.at[owner, half, pl.ds(0, ring - 1)],
-            send_sem=send.at[owner, half],
+            send_sem=send.at[0],
             recv_sem=recv.at[owner, half],
             device_id=in_plane((mine + 1) % ring),
             device_id_type=MESH,
@@ -283,19 +315,19 @@
         return pltpu.make_async_remote_copy(
             src_ref=sums_out.at[owner, half],
             dst_ref=sums_in.at[plane, half],
-            send_sem=sums_send.at[owner, half],
-            recv_sem=sums_recv.at[plane, half],
+            send_sem=sums_send.at[0],
+            recv_sem=sums_recv.at[0],
             device_id=in_line(owner),
             device_id_type=MESH,
         )
 
-    def sums_wait(owner, half):
+    def relay_copy(owner, half):
         return pltpu.make_async_remote_copy(
             src_ref=sums_out.at[owner, half],
-            dst_ref=sums_in.at[owner, half],
-            send_sem=sums_send.at[owner, half],
-            recv_sem=sums_recv.at[owner, half],
-            device_id=in_line(owner),
+            dst_ref=relay_in.at[half],
+            send_sem=sums_send.at[0],
+            recv_sem=relay_recv.at[half],
+            device_id=in_line(plane + 1 - 2 * (plane // (planes - 1))),
             device_id_type=MESH,
         )
 
@@ -316,11 +348,6 @@
 
     places = lax.broadcasted_iota(jnp.int32, (capacity, count), 0).astype(jnp.float32)
 
-    def wait_table(owner):
-        ahead = (owner + planes - plane) % planes
-        for copy in table_copies(ahead, owner):
-            copy.wait_recv()
-
     def dispatch(owner, half):
         @pl.when(owner != plane)
         def _():
@@ -333,10 +360,6 @@
         @pl.when((owner >= plane) & (plane > 0))
         def _():
             rows_copy(owner, half, plane - 1, rows_down).start()
-
-        @pl.when((owner != plane) & (half == 0))
-        def _():
-            wait_table(owner)
 
         slot, _ = slots_of(owner)
         chosen = jnp.concatenate(
@@ -408,6 +431,16 @@
 
     def collect(owner, half):
         block_wait(*back, owner, half).wait_recv()
+        ends = helps = jnp.bool_(False)
+        if relayed:
+            last = planes - 1
+            ends = ((plane == 0) & (owner == last)) | ((plane == last) & (owner == 0))
+            helps = ((plane == 1) & (owner == last)) | ((plane == last - 1) & (owner == 0))
+
+            @pl.when(helps)
+            def _():
+                relay_copy(owner, half).wait_recv()
+
         slot, share = slots_of(owner)
         spread = jnp.concatenate(
             [
@@ -436,13 +469,27 @@
             def _():
                 sums_own[half, :, at : at + step] = value
 
-            @pl.when(owner != plane)
+            @pl.when((owner != plane) & ~helps)
             def _():
                 sums_out[owner, half, :, at : at + step] = value.astype(jnp.bfloat16)
 
-        @pl.when(owner != plane)
+            if relayed:
+
+                @pl.when(helps)
+                def _():
+                    sums_out[owner, half, :, at : at + step] = (
+                        value + relay_in[half, :, at : at + step].astype(jnp.float32)
+                    ).astype(jnp.bfloat16)
+
+        @pl.when((owner != plane) & ~ends)
         def _():
             sums_copy(owner, half).start()
+
+        if relayed:
+
+            @pl.when(ends)
+            def _():
+                relay_copy(owner, half).start()
 
     def share_expert():
         for load in loads[1:4]:
@@ -479,9 +526,56 @@
         load.wait()
     lax.fori_loop(0, len(plans[0]), step, 0)
 
-    for ahead in range(1, planes):
-        for half in range(halves):
-            sums_wait((plane + ahead) % planes, half).wait_recv()
+    for ahead in range(1, tp_count):
+        pltpu.make_async_remote_copy(
+            src_ref=part_out.at[ahead - 1],
+            dst_ref=part_in.at[ahead - 1],
+            send_sem=part_send.at[ahead - 1],
+            recv_sem=part_recv.at[ahead - 1, 0],
+            device_id=(chip, (core + ahead) % tp_count),
+            device_id_type=MESH,
+        ).wait_send()
+    for source, target, send, recv in (go, back):
+        pltpu.make_async_remote_copy(
+            src_ref=source.at[:, :, pl.ds(0, ring - 1)],
+            dst_ref=target.at[:, :, pl.ds(0, ring - 1)],
+            send_sem=send.at[0],
+            recv_sem=recv.at[0, 0],
+            device_id=in_plane((mine + 1) % ring),
+            device_id_type=MESH,
+        ).wait_send()
+
+    def drain(code, carry):
+        owner, half = code // halves, code % halves
+
+        @pl.when((owner <= plane) & (plane < planes - 1))
+        def _():
+            rows_copy(owner, half, plane + 1, rows_up).wait_send()
+
+        @pl.when((owner >= plane) & (plane > 0))
+        def _():
+            rows_copy(owner, half, plane - 1, rows_down).wait_send()
+
+        return carry
+
+    lax.fori_loop(0, planes * halves, drain, 0)
+    if planes > 1:
+        for total_copy in table_totals:
+            total_copy.wait_send()
+        bytes_of(sums_out, planes - 1, sums_send.at[0], sums_recv.at[0]).wait_send()
+        if relayed:
+            at_end = (plane == 0) | (plane == planes - 1)
+
+            @pl.when(at_end)
+            def _():
+                bytes_of(sums_in, planes - 2, sums_send.at[0], sums_recv.at[0]).wait_recv()
+
+            @pl.when(~at_end)
+            def _():
+                bytes_of(sums_in, planes - 1, sums_send.at[0], sums_recv.at[0]).wait_recv()
+
+        else:
+            bytes_of(sums_in, planes - 1, sums_send.at[0], sums_recv.at[0]).wait_recv()
 
     def last_band(number, carry):
         spot = pl.ds(pl.multiple_of(number * band, band), band)
@@ -497,40 +591,13 @@
 
     lax.fori_loop(0, count // band, last_band, 0)
 
-    for ahead in range(1, tp_count):
-        for copy in part_copies(ahead):
-            copy.wait_send()
-    for ahead in range(1, planes):
-        for copy in table_copies(ahead, plane):
-            copy.wait_send()
-
-    def drain(code, carry):
-        owner, half = code // halves, code % halves
-        block_wait(*go, owner, half).wait_send()
-        block_wait(*back, owner, half).wait_send()
-
-        @pl.when(owner != plane)
-        def _():
-            sums_copy(owner, half).wait_send()
-
-        @pl.when((owner <= plane) & (plane < planes - 1))
-        def _():
-            rows_copy(owner, half, plane + 1, rows_up).wait_send()
-
-        @pl.when((owner >= plane) & (plane > 0))
-        def _():
-            rows_copy(owner, half, plane - 1, rows_down).wait_send()
-
-        return carry
-
-    lax.fori_loop(0, planes * halves, drain, 0)
-
 
 def mixer_stage(
     heads,
     groups,
     owners,
     head_dim,
+    gate_ready,
     signal_in,
     write_in,
     read_in,
@@ -647,8 +714,8 @@
         return pltpu.make_async_remote_copy(
             src_ref=decay_out,
             dst_ref=decay_in.at[device],
-            send_sem=decay_send.at[owner],
-            recv_sem=decay_recv.at[device],
+            send_sem=decay_send.at[0],
+            recv_sem=decay_recv.at[0],
             device_id=(owner, core),
             device_id_type=MESH,
         )
@@ -657,7 +724,7 @@
         return pltpu.make_async_remote_copy(
             src_ref=piece_out.at[owner],
             dst_ref=piece_in.at[device],
-            send_sem=piece_send.at[owner],
+            send_sem=piece_send.at[0],
             recv_sem=piece_recv.at[device],
             device_id=(owner, core),
             device_id_type=MESH,
@@ -667,8 +734,8 @@
         return pltpu.make_async_remote_copy(
             src_ref=start_out.at[device],
             dst_ref=start_in.at[owner],
-            send_sem=start_send.at[device],
-            recv_sem=start_recv.at[owner],
+            send_sem=start_send.at[0],
+            recv_sem=start_recv.at[0],
             device_id=(device, core),
             device_id_type=MESH,
         )
@@ -679,6 +746,19 @@
             @pl.when(at != chip)
             def _():
                 act(at)
+
+    def with_others(act):
+        if owners == chips:
+            act(owners - 1)
+        else:
+
+            @pl.when(chip < owners)
+            def _():
+                act(owners - 1)
+
+            @pl.when(chip >= owners)
+            def _():
+                act(owners)
 
     others(owners, lambda owner: decay_copy(owner, chip).start())
 
@@ -695,29 +775,17 @@
     for source, _, _, at, size in parts:
         extended[head_room : head_room + length, at : at + size] = source[...].astype(f32)
 
-    @pl.when(chip > 0)
-    def _():
-        for copy in halo_copies(chip):
-            copy.wait_recv()
-        for _, halo, _, at, size in parts:
-            extended[0:head_room, at : at + size] = halo[rim - head_room : rim, :].astype(f32)
-
-    @pl.when(chip == 0)
-    def _():
-        extended[0:head_room, :] = jnp.zeros((head_room, extended.shape[1]), f32)
-
-    def convolve(weights, at, size, put):
-        for b in range(blocks):
-            for lanes in range(0, size, 256):
-                total = None
-                for tap in range(taps):
-                    begin = head_room - taps + 1 + tap + b * BLK
-                    term = (
-                        weights[tap : tap + 1, lanes : lanes + 256].astype(f32)
-                        * extended[begin : begin + BLK, at + lanes : at + lanes + 256]
-                    )
-                    total = term if total is None else total + term
-                put(b, lanes, jax.nn.silu(total))
+    def convolve(b, weights, at, size, put):
+        for lanes in range(0, size, 256):
+            total = None
+            for tap in range(taps):
+                begin = head_room - taps + 1 + tap + b * BLK
+                term = (
+                    weights[tap : tap + 1, lanes : lanes + 256].astype(f32)
+                    * extended[begin : begin + BLK, at + lanes : at + lanes + 256]
+                )
+                total = term if total is None else total + term
+            put(b, lanes, jax.nn.silu(total))
 
     def put_write(b, lanes, value):
         write_vec[b * BLK : (b + 1) * BLK, lanes : lanes + 256] = value.astype(bf16)
@@ -728,9 +796,9 @@
     def put_signal(b, lanes, value):
         signal[b * BLK : (b + 1) * BLK, lanes : lanes + 256] = value
 
-    convolve(write_taps, wide, narrow, put_write)
-    convolve(signal_taps, 0, wide, put_signal)
-    for b in range(blocks):
+    def state_of(b):
+        convolve(b, write_taps, wide, narrow, put_write)
+        convolve(b, signal_taps, 0, wide, put_signal)
         spot = slice(b * BLK, (b + 1) * BLK)
         step = timestep[spot]
         scaled[spot, :] = (signal[spot, :] * expand(step)).astype(bf16)
@@ -743,22 +811,12 @@
                 (((0,), (0,)), ((), ())),
                 preferred_element_type=f32,
             )
-    for owner in range(owners):
-        spot = slice(owner * rows, (owner + 1) * rows)
-        value = states[0, spot, :]
-        for b in range(1, blocks):
-            value = value * readout[(b + 1) * BLK - 1 : (b + 1) * BLK, :] + states[b, spot, :]
-        piece_out[owner] = value.astype(bf16)
-    others(owners, lambda owner: piece_copy(owner, chip).start())
-
-    @pl.when(chip < owners)
-    def _():
-        piece_in[chip] = piece_out[chip]
-
-    convolve(read_taps, wide + narrow, narrow, put_read)
+
     spread_direct = expand(jnp.broadcast_to(direct[...], (8, heads)))[0:1, :]
     low_lanes = lax.broadcasted_iota(jnp.int32, (BLK, 2 * head_dim), 1) < head_dim
-    for b in range(blocks):
+
+    def within(b):
+        convolve(b, read_taps, wide + narrow, narrow, put_read)
         spot = slice(b * BLK, (b + 1) * BLK)
         turned = cums[b].T
         for g in range(groups):
@@ -787,12 +845,43 @@
                     jnp.concatenate(weights, axis=1), both, preferred_element_type=f32
                 )
 
+    for b in range(1, blocks):
+        state_of(b)
+        within(b)
+
+    @pl.when(chip > 0)
+    def _():
+        for copy in halo_copies(chip):
+            copy.wait_recv()
+        for _, halo, _, at, size in parts:
+            extended[0:head_room, at : at + size] = halo[rim - head_room : rim, :].astype(f32)
+
+    @pl.when(chip == 0)
+    def _():
+        extended[0:head_room, :] = jnp.zeros((head_room, extended.shape[1]), f32)
+
+    state_of(0)
+    for owner in range(owners):
+        spot = slice(owner * rows, (owner + 1) * rows)
+        value = states[0, spot, :]
+        for b in range(1, blocks):
+            value = value * readout[(b + 1) * BLK - 1 : (b + 1) * BLK, :] + states[b, spot, :]
+        piece_out[owner] = value.astype(bf16)
+    others(owners, lambda owner: piece_copy(owner, chip).start())
+
     @pl.when(chip < owners)
     def _():
+        piece_in[chip] = piece_out[chip]
+
+    within(0)
+
+    @pl.when(chip < owners)
+    def _():
+        bytes_of(decay_in, chips - 1, decay_send.at[0], decay_recv.at[0]).wait_recv()
+
         def scan(device, held):
             @pl.when(device != chip)
             def _():
-                decay_copy(chip, device).wait_recv()
                 piece_copy(chip, device).wait_recv()
 
             start_out[device] = held.astype(bf16)
@@ -806,7 +895,10 @@
         lax.fori_loop(0, chips, scan, jnp.zeros((rows, wide), f32))
         start_in[chip] = start_out[chip]
 
-    others(owners, lambda owner: start_copy(owner, chip).wait_recv())
+    with_others(
+        lambda number: bytes_of(start_in, number, start_send.at[0], start_recv.at[0]).wait_recv()
+    )
+    gate_ready()
     start = jnp.concatenate([start_in[owner].astype(f32) for owner in range(owners)], axis=0)
     for b in range(blocks):
         spot = slice(b * BLK, (b + 1) * BLK)
@@ -832,12 +924,16 @@
         for copy in halo_copies(chip + 1):
             copy.wait_send()
 
-    others(owners, lambda owner: decay_copy(owner, chip).wait_send())
-    others(owners, lambda owner: piece_copy(owner, chip).wait_send())
+    with_others(
+        lambda number: bytes_of(decay_in, number, decay_send.at[0], decay_recv.at[0]).wait_send()
+    )
+    with_others(
+        lambda number: bytes_of(piece_out, number, piece_send.at[0], piece_recv.at[0]).wait_send()
+    )
 
     @pl.when(chip < owners)
     def _():
-        others(chips, lambda device: start_copy(chip, device).wait_send())
+        bytes_of(start_out, chips - 1, start_send.at[0], start_recv.at[0]).wait_send()
 
 
 def mixer_scratch(chips, owners, length, wide, narrow, blocks):
@@ -866,25 +962,31 @@
         pltpu.VMEM((owners, rows, wide), bf16),
         dma((3,)),
         dma((3,)),
-        dma((owners,)),
+        dma((1,)),
         dma((chips,)),
-        dma((owners,)),
-        dma((chips,)),
-        dma((chips,)),
-        dma((owners,)),
+        dma((1,)),
+        dma((1,)),
+        dma((1,)),
+        dma((1,)),
     ]
 
 
 def layer_kernel(tail_sizes, mixer_sizes, mixer_scratch_count, *refs):
     mixer_in, tail_in, out = refs[:13], refs[13:24], refs[24]
-    mixed = refs[25]
-    mixer_refs = refs[26 : 26 + mixer_scratch_count]
-    tail_refs = refs[26 + mixer_scratch_count :]
+    mixed, gate_held, stream_held, early_sem = refs[25:29]
+    mixer_refs = refs[29 : 29 + mixer_scratch_count]
+    tail_refs = refs[29 + mixer_scratch_count :]
+    gate_load = pltpu.make_async_copy(mixer_in[3], gate_held, early_sem.at[0])
+    stream_load = pltpu.make_async_copy(tail_in[0], stream_held, early_sem.at[1])
+    gate_load.start()
+    stream_load.start()
+    held_in = (*mixer_in[:3], gate_held, *mixer_in[4:])
 
     def mix():
-        mixer_stage(*mixer_sizes, *mixer_in, mixed, *mixer_refs)
-
-    tail_stage(*tail_sizes, mix, mixed, *tail_in, out, *tail_refs)
+        mixer_stage(*mixer_sizes, gate_load.wait, *held_in, mixed, *mixer_refs)
+        stream_load.wait()
+
+    tail_stage(*tail_sizes, mix, mixed, stream_held, *tail_in[1:], out, *tail_refs)
 
 
 def layer(mixer_in, tail_in):
@@ -917,11 +1019,14 @@
             mixer_sizes,
             len(mixer_refs),
         ),
-        out_shape=jax.ShapeDtypeStruct((count, width), bf16),
-        in_specs=[vmem] * 17 + [anywhere] * 7,
+        out_shape=pltpu.VMEM((count, width), bf16),
+        in_specs=[vmem] * 3 + [anywhere] + [vmem] * 9 + [anywhere] + [vmem] * 3 + [anywhere] * 7,
         out_specs=vmem,
         scratch_shapes=[
             pltpu.VMEM((length, wide), bf16),
+            pltpu.VMEM((length, wide), bf16),
+            pltpu.VMEM((count, width), bf16),
+            dma((2,)),
             *mixer_refs,
             pltpu.VMEM(out_weight.shape, bf16),
             pltpu.VMEM(gate.shape[1:], bf16),
@@ -947,12 +1052,20 @@
             pltpu.VMEM(pieces[1:], f32),
             pltpu.VMEM(pieces, bf16),
             pltpu.VMEM(pieces, bf16),
+            pltpu.VMEM(pieces[1:], bf16),
             dma((7,)),
+            dma((tp_count - 1,)),
             dma((tp_count - 1, chunks)),
-            dma((tp_count - 1, chunks)),
-            dma((2, planes)),
-            dma((2, planes)),
-            *[dma((planes, HALVES))] * 9,
+            dma((2,)),
+            dma((2,)),
+            *[dma((planes, HALVES))] * 3,
+            dma((1,)),
+            dma((planes, HALVES)),
+            dma((1,)),
+            dma((planes, HALVES)),
+            dma((1,)),
+            dma((1,)),
+            dma((HALVES,)),
         ],
         compiler_params=pltpu.CompilerParams(
             collective_id=0, has_side_effects=True, vmem_limit_bytes=62 * 2**20

time: 121 us -> 114 us (0.942)
  Pallas kernels: 119 us -> 113 us
    pallas_call x1, Pallas kernels: 119 us -> 113 us  [layer(): pl.pallas_call(functools.partial(layer_kernel, (planes, ring, tp_count, c...]
where the time goes in v5:
time: 114 us
  Pallas kernels  113 us (99%)
    pallas_call x1, Pallas kernels, layer(): pl.pallas_call(functools.partial(layer_kernel, (planes, ring, tp_count, c...  113 us

profile of v5, /device:TPU:0, one launch (start us, length us, event | category | flops | bytes accessed | tf_op | source)
XLA Modules:
  0.0 113.5 jit_solution(9759379163695119733)
XLA Ops:
  0.0 112.7 %shard_map.226 = bf16[128,2048]{1,0:T(8,128)(2,1)S(1)} custom-call(bf16[256,1024]{1,0:T(8,128)(2,1)} %refs_0_.1, bf16[256,256]{1,0:T(8,128)(2,1)} %refs_1_.1, bf16[256,256]{1,0:T(8,128)(2,1)} %refs_2_.1, bf16[256,1024]{1,0:T(8,128)(2,1)} %refs_3_.1, bf16[16,256]{1,0:T(8,128)(2,1)} %bitcast.10, f32[16,256]{1,0:T(8,128)} %bitcast.9, bf16[4,1024]{1,0:T(4,128)(2,1)} %refs_6_.1, ...), custom_call_target="tpu_custom_call" | custom-call | tf_op jit(solution)/shard_map/pallas_call | solution.py:1015
  112.7 0.8 copy.26

commit v6 on v5

--- a/solution.py
+++ b/solution.py
@@ -83,7 +83,7 @@
     tp_count,
     capacity,
     fanout,
-    mix,
+    steps,
     mixed_ref,
     stream_ref,
     gain_ref,
@@ -168,9 +168,6 @@
             ]
         )
     ]
-    for load in loads:
-        load.start()
-
     barrier = pltpu.get_barrier_semaphore()
     all_chips = lax.axis_size("sp")
     for ahead in range(1, all_chips):
@@ -185,7 +182,12 @@
                 device_id=(plane * chips + spot, (core + ahead) % tp_count),
                 device_id_type=MESH,
             )
+    load_inputs, inputs_ready, mix = steps
+    load_inputs()
+    for load in loads:
+        load.start()
     pl.semaphore_wait(barrier, all_chips - 1 + chips * (tp_count - 1))
+    inputs_ready()
 
     def table_copies(ahead, owner):
         return [
@@ -275,7 +277,7 @@
             rows[plane, half, spot, :] = value[:, half * part : (half + 1) * part]
         return carry
 
-    lax.fori_loop(0, count // band, norm_band, 0)
+    lax.fori_loop(0, count // band, norm_band, 0, unroll=2)
 
     def rows_copy(owner, half, target, sem):
         return pltpu.make_async_remote_copy(
@@ -973,20 +975,31 @@
 
 def layer_kernel(tail_sizes, mixer_sizes, mixer_scratch_count, *refs):
     mixer_in, tail_in, out = refs[:13], refs[13:24], refs[24]
-    mixed, gate_held, stream_held, early_sem = refs[25:29]
-    mixer_refs = refs[29 : 29 + mixer_scratch_count]
-    tail_refs = refs[29 + mixer_scratch_count :]
-    gate_load = pltpu.make_async_copy(mixer_in[3], gate_held, early_sem.at[0])
-    stream_load = pltpu.make_async_copy(tail_in[0], stream_held, early_sem.at[1])
-    gate_load.start()
-    stream_load.start()
-    held_in = (*mixer_in[:3], gate_held, *mixer_in[4:])
+    mixed, early_sem = refs[25:27]
+    held, refs = refs[27:44], refs[44:]
+    mixer_refs, tail_refs = refs[:mixer_scratch_count], refs[mixer_scratch_count:]
+    early = [
+        pltpu.make_async_copy(source, target, early_sem.at[number])
+        for number, (source, target) in enumerate(zip((*mixer_in, *tail_in[:4]), held))
+    ]
+    late = (3, 13, 14)
+
+    def load_inputs():
+        for number in sorted(range(17), key=lambda number: number in late):
+            early[number].start()
+
+    def inputs_ready():
+        for number in range(17):
+            if number not in late:
+                early[number].wait()
 
     def mix():
-        mixer_stage(*mixer_sizes, gate_load.wait, *held_in, mixed, *mixer_refs)
-        stream_load.wait()
-
-    tail_stage(*tail_sizes, mix, mixed, stream_held, *tail_in[1:], out, *tail_refs)
+        mixer_stage(*mixer_sizes, early[3].wait, *held[:13], mixed, *mixer_refs)
+        early[13].wait()
+        early[14].wait()
+
+    steps = (load_inputs, inputs_ready, mix)
+    tail_stage(*tail_sizes, steps, mixed, *held[13:], *tail_in[4:], out, *tail_refs)
 
 
 def layer(mixer_in, tail_in):
@@ -1020,13 +1033,12 @@
             len(mixer_refs),
         ),
         out_shape=pltpu.VMEM((count, width), bf16),
-        in_specs=[vmem] * 3 + [anywhere] + [vmem] * 9 + [anywhere] + [vmem] * 3 + [anywhere] * 7,
+        in_specs=[anywhere] * 24,
         out_specs=vmem,
         scratch_shapes=[
             pltpu.VMEM((length, wide), bf16),
-            pltpu.VMEM((length, wide), bf16),
-            pltpu.VMEM((count, width), bf16),
-            dma((2,)),
+            dma((17,)),
+            *[pltpu.VMEM(part.shape, part.dtype) for part in (*mixer_in, *tail_in[:4])],
             *mixer_refs,
             pltpu.VMEM(out_weight.shape, bf16),
             pltpu.VMEM(gate.shape[1:], bf16),

time: 114 us -> 113 us (level)
  no operation moved by 1% of the time
where the time goes in v6:
time: 113 us
  Pallas kernels  112 us (99%)
    pallas_call x1, Pallas kernels, layer(): pl.pallas_call(functools.partial(layer_kernel, (planes, ring, tp_count, c...  112 us

profile of v6, /device:TPU:0, one launch (start us, length us, event | category | flops | bytes accessed | tf_op | source)
XLA Modules:
  0.0 112.5 jit_solution(8888072153010948337)
XLA Ops:
  0.0 111.7 %shard_map.226 = bf16[128,2048]{1,0:T(8,128)(2,1)S(1)} custom-call(bf16[256,1024]{1,0:T(8,128)(2,1)} %refs_0_.1, bf16[256,256]{1,0:T(8,128)(2,1)} %refs_1_.1, bf16[256,256]{1,0:T(8,128)(2,1)} %refs_2_.1, bf16[256,1024]{1,0:T(8,128)(2,1)} %refs_3_.1, bf16[16,256]{1,0:T(8,128)(2,1)} %bitcast.10, f32[16,256]{1,0:T(8,128)} %bitcast.9, bf16[4,1024]{1,0:T(4,128)(2,1)} %refs_6_.1, ...), custom_call_target="tpu_custom_call" | custom-call | tf_op jit(solution)/shard_map/pallas_call | solution.py:1028
  111.7 0.8 copy.26

commit v7 on v6

--- a/solution.py
+++ b/solution.py
@@ -13,37 +13,38 @@
 
 MESH = pl.DeviceIdType.MESH
 PLANES = 4
-HALVES = 2
+PARTS = 4
 COLS = 512
 
 
 LINE_END = [
-    (0, 0, 0), (0, 0, 1), (0, 1, 0), (0, 1, 1), (0, 2, 0), (0, 2, 1),
-    (0, 3, 0), (1, 2, 0), (2, 2, 0), (0, 3, 1), (2, 2, 1), (3, 0, 0),
-    (1, 3, 0), (2, 3, 0), (1, 1, 0), (1, 0, 0), (2, 3, 1), (2, 1, 0),
-    (2, 1, 1), (2, 0, 0), (2, 0, 1),
+    (0, 0, 0), (3, 0, 0), (0, 0, 1), (0, 0, 2), (0, 0, 3), (0, 1, 0),
+    (0, 1, 1), (0, 2, 0), (0, 2, 1), (0, 3, 0), (0, 3, 1), (0, 3, 2),
+    (0, 3, 3), (0, 1, 2), (1, 3, 0), (0, 2, 2), (2, 3, 0), (0, 2, 3),
+    (2, 3, 1), (0, 1, 3), (2, 3, 2), (2, 3, 3), (1, 2, 0), (1, 1, 0),
+    (2, 2, 0), (2, 2, 1), (2, 2, 2), (1, 0, 0), (2, 2, 3), (2, 1, 0),
+    (2, 1, 1), (2, 1, 2), (2, 0, 0), (2, 1, 3), (2, 0, 1), (2, 0, 2),
+    (2, 0, 3),
 ]
 LINE_NEXT = [
-    (0, 1, 0), (0, 1, 1), (3, 1, 0), (0, 0, 0), (0, 2, 0), (0, 2, 1),
-    (0, 3, 0), (0, 0, 1), (1, 2, 0), (1, 0, 0), (0, 3, 1), (1, 1, 0),
-    (2, 0, 0), (2, 2, 0), (1, 3, 0), (2, 1, 0), (2, 2, 1), (2, 0, 1),
-    (2, 3, 0), (2, 3, 1), (2, 1, 1),
+    (0, 1, 0), (0, 1, 1), (0, 2, 0), (0, 0, 0), (0, 2, 1), (0, 0, 1),
+    (0, 3, 0), (0, 0, 2), (0, 3, 1), (0, 0, 3), (0, 3, 2), (0, 3, 3),
+    (0, 1, 2), (1, 0, 0), (0, 2, 2), (0, 1, 3), (0, 2, 3), (1, 3, 0),
+    (2, 0, 0), (1, 2, 0), (2, 3, 0), (2, 3, 1), (3, 1, 0), (2, 3, 2),
+    (2, 3, 3), (2, 0, 1), (2, 2, 0), (1, 1, 0), (2, 2, 1), (2, 1, 0),
+    (2, 0, 2), (2, 2, 2), (2, 1, 1), (2, 2, 3), (2, 0, 3), (2, 1, 2),
+    (2, 1, 3),
 ]
 
 
-def line_plans(planes, halves):
-    if (planes, halves) == (4, 2):
-        mirror = lambda plan: [(kind, 3 - owner, half) for kind, owner, half in plan]
-        plans = [LINE_END, LINE_NEXT, mirror(LINE_NEXT), mirror(LINE_END)]
-    else:
-        plans = []
-        for z in range(planes):
-            near = sorted(range(planes), key=lambda s: (abs(s - z), s))
-            plan = [(0, s, h) for s in near for h in range(halves)] + [(3, 0, 0)]
-            for s in near:
-                plan += [(1, s, 0)] + [(2, s, h) for h in range(halves)]
-            plans.append(plan)
-    return [[(k * planes + s) * halves + h for k, s, h in plan] for plan in plans]
+def line_plans(planes, parts):
+    code = lambda plan: [(k * planes + s) * parts + h for k, s, h in plan]
+    if (planes, parts) == (4, 4):
+        return [code(LINE_END), code(LINE_NEXT)]
+    plan = [(0, s, h) for s in range(planes) for h in range(parts)] + [(3, 0, 0)]
+    for s in range(planes):
+        plan += [(1, s, 0)] + [(2, s, h) for h in range(parts)]
+    return [code(plan)] * 2
 
 
 def column_chunks(width):
@@ -51,17 +52,10 @@
     return [(at, step) for at in range(0, width, step)]
 
 
-def pick(values, place, which):
+def pick(plans, inner, turn):
     chosen = jnp.int32(0)
-    for spot, row in enumerate(values):
-        chosen = chosen + (place == spot).astype(jnp.int32) * pick_one(row, which)
-    return chosen
-
-
-def pick_one(row, which):
-    chosen = jnp.int32(0)
-    for spot, value in enumerate(row):
-        chosen = chosen + (which == spot).astype(jnp.int32) * value
+    for spot, (end, near) in enumerate(zip(*plans)):
+        chosen = chosen + (turn == spot).astype(jnp.int32) * (end + inner * (near - end))
     return chosen
 
 
@@ -147,6 +141,7 @@
     halves = rows.shape[1]
     part = width // halves
     plans = line_plans(planes, halves)
+    relayed = planes == 4
 
     def in_plane(spot):
         return (plane * chips + spot // tp_count, spot % tp_count)
@@ -209,14 +204,13 @@
             copy.start()
     index_tables[plane] = index_ref[...]
     weight_tables[plane] = weight_ref[...]
-    relayed = planes == 4
     if relayed:
 
-        @pl.when(plane == 0)
+        @pl.when(plane == 1)
         def _():
-            sums_in[planes - 1] = jnp.zeros(sums_in.shape[1:], jnp.bfloat16)
-
-        @pl.when(plane == planes - 1)
+            sums_in[3] = jnp.zeros(sums_in.shape[1:], jnp.bfloat16)
+
+        @pl.when(plane == 2)
         def _():
             sums_in[0] = jnp.zeros(sums_in.shape[1:], jnp.bfloat16)
 
@@ -435,9 +429,8 @@
         block_wait(*back, owner, half).wait_recv()
         ends = helps = jnp.bool_(False)
         if relayed:
-            last = planes - 1
-            ends = ((plane == 0) & (owner == last)) | ((plane == last) & (owner == 0))
-            helps = ((plane == 1) & (owner == last)) | ((plane == last - 1) & (owner == 0))
+            ends = ((plane == 0) & (owner == 2)) | ((plane == 3) & (owner == 1))
+            helps = ((plane == 1) & (owner == 2)) | ((plane == 2) & (owner == 1))
 
             @pl.when(helps)
             def _():
@@ -503,8 +496,10 @@
         ffn(normed, common_gate, common_up, common_down, residual, put)
 
     def step(turn, carry):
-        code = pick(plans, plane, turn)
+        code = pick(plans, (plane + 1) // 2 % 2, turn)
         half, owner, kind = code % halves, code // halves % planes, code // (halves * planes)
+        if relayed:
+            owner = owner + plane // 2 * (planes - 1 - 2 * owner)
 
         @pl.when(kind == 0)
         def _():
@@ -566,13 +561,13 @@
             total_copy.wait_send()
         bytes_of(sums_out, planes - 1, sums_send.at[0], sums_recv.at[0]).wait_send()
         if relayed:
-            at_end = (plane == 0) | (plane == planes - 1)
-
-            @pl.when(at_end)
+            inside = (plane == 1) | (plane == 2)
+
+            @pl.when(inside)
             def _():
                 bytes_of(sums_in, planes - 2, sums_send.at[0], sums_recv.at[0]).wait_recv()
 
-            @pl.when(~at_end)
+            @pl.when(~inside)
             def _():
                 bytes_of(sums_in, planes - 1, sums_send.at[0], sums_recv.at[0]).wait_recv()
 
@@ -1021,10 +1016,10 @@
     experts = sp_count * tp_count
     capacity = max(2, (3 * count * fanout + 2 * experts - 1) // (2 * experts))
     capacity = (capacity + 7) // 8 * 8
-    part = width // HALVES
+    part = width // PARTS
     chunks = len(column_chunks(width))
-    slots = (planes, HALVES, ring, capacity, part)
-    pieces = (planes, HALVES, count, part)
+    slots = (planes, PARTS, ring, capacity, part)
+    pieces = (planes, PARTS, count, part)
     return pl.pallas_call(
         functools.partial(
             layer_kernel,
@@ -1070,14 +1065,14 @@
             dma((tp_count - 1, chunks)),
             dma((2,)),
             dma((2,)),
-            *[dma((planes, HALVES))] * 3,
+            *[dma((planes, PARTS))] * 3,
             dma((1,)),
-            dma((planes, HALVES)),
+            dma((planes, PARTS)),
             dma((1,)),
-            dma((planes, HALVES)),
+            dma((planes, PARTS)),
             dma((1,)),
             dma((1,)),
-            dma((HALVES,)),
+            dma((PARTS,)),
         ],
         compiler_params=pltpu.CompilerParams(
             collective_id=0, has_side_effects=True, vmem_limit_bytes=62 * 2**20

time: 113 us -> 108 us (0.956)
  Pallas kernels: 112 us -> 107 us
    pallas_call x1, Pallas kernels: 112 us -> 107 us  [layer(): pl.pallas_call(functools.partial(layer_kernel, (planes, ring, tp_count, c...]
where the time goes in v7:
time: 108 us
  Pallas kernels  107 us (99%)
    pallas_call x1, Pallas kernels, layer(): pl.pallas_call(functools.partial(layer_kernel, (planes, ring, tp_count, c...  107 us

profile of v7, /device:TPU:0, one launch (start us, length us, event | category | flops | bytes accessed | tf_op | source)
XLA Modules:
  0.0 107.5 jit_solution(11214788699151291658)
XLA Ops:
  0.0 106.7 %shard_map.226 = bf16[128,2048]{1,0:T(8,128)(2,1)S(1)} custom-call(bf16[256,1024]{1,0:T(8,128)(2,1)} %refs_0_.1, bf16[256,256]{1,0:T(8,128)(2,1)} %refs_1_.1, bf16[256,256]{1,0:T(8,128)(2,1)} %refs_2_.1, bf16[256,1024]{1,0:T(8,128)(2,1)} %refs_3_.1, bf16[16,256]{1,0:T(8,128)(2,1)} %bitcast.10, f32[16,256]{1,0:T(8,128)} %bitcast.9, bf16[4,1024]{1,0:T(4,128)(2,1)} %refs_6_.1, ...), custom_call_target="tpu_custom_call" | custom-call | tf_op jit(solution)/shard_map/pallas_call | solution.py:1023
  106.7 0.8 copy.26
